TPU v7x, 32 devices: a whole 2x2x4 slice. The times are simulated.
32 devices in a mesh: rep: 8 (over z, y), fs: 2 (over x), tp: 2 (over core).
Axes of the slice: x: 2, y: 2, z: 4, core: 2. Of those that a mesh axis runs over, the one named last changes fastest.
Arguments:
- tokens: bfloat16 [8192, 1024], P(('rep', 'fs', 'tp')), may hold values from -6 to 6
- cotangent: bfloat16 [8192, 1024], P(('rep', 'fs', 'tp')), may hold values from -8 to 8
- gate_weight: bfloat16 [1024, 2816], P(None, ('fs', 'tp')), may hold values from -0.1875 to 0.1875
- value_weight: bfloat16 [1024, 2816], P(None, ('fs', 'tp')), may hold values from -0.1875 to 0.1875
- down_weight: bfloat16 [2816, 1024], P(('fs', 'tp')), may hold values from -0.109375 to 0.109375
- gate_taps: float32 [3, 2816], P(None, ('fs', 'tp')), may hold values from -3.5 to 3.5
- value_taps: float32 [3, 2816], P(None, ('fs', 'tp')), may hold values from -3.5 to 3.5
Outputs:
- input_grad: bfloat16 [8192, 1024], P(('rep', 'fs', 'tp'))
- gate_grad: float32 [1024, 2816], P(None, ('fs', 'tp'))
- value_grad: float32 [1024, 2816], P(None, ('fs', 'tp'))
- down_grad: float32 [2816, 1024], P(('fs', 'tp'))
- gate_taps_grad: float32 [3, 2816], P(None, ('fs', 'tp'))
- value_taps_grad: float32 [3, 2816], P(None, ('fs', 'tp'))
All inputs are finite; a program needn't handle non-finite values.
Results may differ from a plain program's by a relative error of at most 0.0062.
Values may be sent and summed in bfloat16 or wider, within the bound.
No kernel may reach another device: no remote copies, remote signals or barrier semaphores. Data moves between devices by JAX's collectives and lax.ppermute only.
A program may use at most 128 MiB of HBM per device.

v0:
```python
import math

import jax
import jax.numpy as jnp
from jax import lax
from jax.sharding import PartitionSpec as P


def shift_back(field, offset):
    return jnp.pad(field, ((offset, 0), (0, 0)))[: field.shape[0]]


def shift_ahead(field, offset):
    return jnp.pad(field, ((0, offset), (0, 0)))[offset:]


def causal_mix(field, taps):
    total = taps[0][None, :] * field
    for offset in range(1, taps.shape[0]):
        total = total + taps[offset][None, :] * shift_back(field, offset)
    return total


def reverse_mix(field, taps):
    total = taps[0][None, :] * field
    for offset in range(1, taps.shape[0]):
        total = total + taps[offset][None, :] * shift_ahead(field, offset)
    return total


def tap_sums(back, field, count):
    return jnp.stack([jnp.sum(back * shift_back(field, offset), axis=0) for offset in range(count)])


def contract_rows(left, right):
    return lax.dot_general(
        left, right, (((0,), (0,)), ((), ())), preferred_element_type=jnp.float32
    )


def contract_cols(left, right):
    return lax.dot_general(
        left, right, (((1,), (1,)), ((), ())), preferred_element_type=jnp.float32
    )


def per_device(tokens, cotangent, gate_weight, value_weight, down_weight, gate_taps, value_taps):
    local_rows = tokens.shape[0]
    hidden_cols = gate_weight.shape[1]
    seq_len = local_rows * lax.axis_size("fs") * lax.axis_size("tp")
    total_tokens = seq_len * lax.axis_size("rep")
    scale = 1.0 / math.sqrt(total_tokens)
    both_weights = jnp.concatenate([gate_weight, value_weight], axis=1)
    piece = lax.all_gather(tokens, ("fs", "tp"), axis=0, tiled=True)
    whole = piece
    block = jnp.dot(piece, both_weights, preferred_element_type=jnp.float32).astype(jnp.bfloat16)
    projected = block
    token_whole, projected = (whole, projected)
    piece = lax.all_gather(cotangent, ("fs", "tp"), axis=0, tiled=True)
    whole = piece
    back = contract_cols(piece, down_weight)
    up_gate = projected[:, :hidden_cols].astype(jnp.float32)
    up_value = projected[:, hidden_cols:].astype(jnp.float32)
    conv_gate = causal_mix(up_gate, gate_taps)
    conv_value = causal_mix(up_value, value_taps)
    sigma = jax.nn.sigmoid(conv_gate)
    silu_gate = conv_gate * sigma
    hidden = (silu_gate * conv_value).astype(jnp.bfloat16)
    back_value = back * silu_gate
    back_gate = back * conv_value * sigma * (1.0 + conv_gate * (1.0 - sigma))
    grad_gate = reverse_mix(back_gate, gate_taps).astype(jnp.bfloat16)
    grad_value = reverse_mix(back_value, value_taps).astype(jnp.bfloat16)
    tap_count = gate_taps.shape[0]
    input_grad = lax.psum_scatter(
        contract_cols(grad_gate, gate_weight) + contract_cols(grad_value, value_weight),
        ("fs", "tp"),
        scatter_dimension=0,
        tiled=True,
    ).astype(jnp.bfloat16)
    gate_part = contract_rows(token_whole, grad_gate)
    value_part = contract_rows(token_whole, grad_value)
    down_part = contract_rows(hidden, whole)
    gate_tap_part = tap_sums(back_gate, up_gate, tap_count)
    value_tap_part = tap_sums(back_value, up_value, tap_count)
    summed = lax.psum((gate_part, value_part, down_part, gate_tap_part, value_tap_part), "rep")
    weight_out = tuple((item * scale for item in summed))
    return (input_grad, weight_out[0], weight_out[1], weight_out[2], weight_out[3], weight_out[4])


def solution(mesh):
    in_specs = (
        P(("rep", "fs", "tp"), None),
        P(("rep", "fs", "tp"), None),
        P(None, ("fs", "tp")),
        P(None, ("fs", "tp")),
        P(("fs", "tp"), None),
        P(None, ("fs", "tp")),
        P(None, ("fs", "tp")),
    )
    out_specs = (
        P(("rep", "fs", "tp"), None),
        P(None, ("fs", "tp")),
        P(None, ("fs", "tp")),
        P(("fs", "tp"), None),
        P(None, ("fs", "tp")),
        P(None, ("fs", "tp")),
    )
    return jax.shard_map(
        per_device, mesh=mesh, in_specs=in_specs, out_specs=out_specs, check_vma=False
    )
```

profile of v0, /device:TPU:0, one launch (start us, length us, event | category | flops | bytes accessed | tf_op | source)
XLA Modules:
  0.0 440.8 jit_solution(10589605548296215302)
XLA Ops:
  7.2 0.0 copy-start
  7.2 0.0 all-gather.5.cloned.1.call-start
  7.2 0.7 all-gather.5.cloned.1.call-update
  7.9 0.0 all-gather.3.cloned.1.call-start
  8.0 0.7 all-gather.3.cloned.1.call-update
  8.7 0.0 reduce-scatter.2.cloned.1.call-start
  8.7 0.8 slice_reduce_fusion.5
  9.6 0.8 slice_reduce_fusion.4
  10.4 24.5 %all-gather.5.cloned.1.call-done = bf16[1024,1024]{1,0:T(8,128)(2,1)} async-done(((bf16[256,1024]{1,0:T(8,128)(2,1)}), bf16[1024,1024]{1,0:T(8,128)(2,1)}) %all-gather.5.cloned.1.call-update) | async-done | bytes 2097168 | tf_op jit(solution)/shard_map/all_gather | solution.py:54
  34.9 5.7 %fusion = bf16[1024,1408]{0,1:T(8,128)(2,1)S(1)} fusion(bf16[1024,1024]{1,0:T(8,128)(2,1)} %all-gather.5.cloned.1.call-done, bf16[1024,704]{0,1:T(8,128)(2,1)} %param.10, bf16[1024,704]{0,1:T(8,128)(2,1)} %param.9), kind=kOutput, calls=%fused_computation.1 | convolution fusion | flops 2959998976 | bytes 7864320 | tf_op jit(solution)/shard_map/dot_general | solution.py:56
  40.5 0.0 copy-start.4
  40.5 1.6 copy-done.4
  42.1 3.2 slice_convert_fusion.1
  45.3 13.7 %all-gather.3.cloned.1.call-done = bf16[1024,1024]{1,0:T(8,128)(2,1)} async-done(((bf16[256,1024]{1,0:T(8,128)(2,1)}), bf16[1024,1024]{1,0:T(8,128)(2,1)}) %all-gather.3.cloned.1.call-update) | async-done | bytes 2097168 | tf_op jit(solution)/shard_map/all_gather | solution.py:59
  59.0 0.0 copy-done
  59.0 23.6 %multiply_reduce_fusion.2 = (f32[704]{0:T(1024)S(1)}, f32[704]{0:T(1024)S(1)}, f32[704]{0:T(1024)S(1)}, f32[704]{0:T(1024)S(1)}, f32[704]{0:T(1024)S(1)}, /*inde...) fusion(bf16[1024,1408]{0,1:T(8,128)(2,1)} %copy-done.4, ...), kind=kOutput, calls=%fused_computation.25 | convolution fusion | flops 1501621760 | bytes 23757824 | tf_op jit(solution)/shard_map/dot_general | solution.py:42
  82.7 0.0 copy-start.7
  82.7 11.0 %fusion.4 = (bf16[1024,704]{0,1:T(8,128)(2,1)S(1)}, bf16[1024,704]{0,1:T(8,128)(2,1)S(1)}) fusion(f32[1024,704]{0,1:T(8,128)} %get-tuple-element.28, f32[704]{0:T(1024)S(1)} %get-tuple-element.20, f32[704]{0:T(1024)S(1)} %get-tuple-element.21, f32[704]{0:T(1024)S(1)} %get-tuple-element.19, f32[1024,704]{0,1:T(8,128)} %get-tuple-element.27, ...), kind=kLoop, calls=%fused_computation.13 | loop fusion | flops 8650752 | bytes 8667648 | tf_op jit(solution)/shard_map/convert_element_type | solution.py:71
  93.7 0.0 copy-done.7
  93.7 0.0 copy-start.8
  93.7 1.9 fusion.21
  95.6 0.0 copy-done.8
  95.6 3.8 convolution_add_fusion
  99.4 0.0 reduce-scatter.2.cloned.1.call-update
  99.5 0.2 all-reduce.12.cloned.1.call-start
  99.7 0.0 copy-start.5
  99.7 5.0 %convolution_bitcast_fusion.1 = f32[1024,704]{0,1:T(8,128)} fusion(bf16[1024,704]{0,1:T(8,128)(2,1)S(1)} %get-tuple-element.33, bf16[1024,1024]{1,0:T(8,128)(2,1)} %all-gather.5.cloned.1.call-done), kind=kOutput, calls=%fused_computation.37 | convolution fusion | flops 1476395008 | bytes 6422528 | tf_op jit(solution)/shard_map/dot_general | solution.py:36
  104.7 0.0 copy-done.5
  104.7 0.0 copy-start.6
  104.7 0.0 copy-start.9
  104.7 0.0 copy-start.10
  104.7 3.3 convolution_bitcast_fusion
  108.0 0.0 copy-done.6
  108.0 0.0 copy-done.9
  108.0 1.6 copy-done.10
  109.7 3.3 fusion.15
  113.0 0.0 all-reduce.12.cloned.1.call-update
  113.1 37.6 %all-reduce.8 = (f32[3,704]{1,0:T(4,128)S(1)}, f32[3,704]{1,0:T(4,128)S(1)}) all-reduce(f32[3,704]{1,0:T(4,128)S(1)} %pad_maximum_fusion, f32[3,704]{1,0:T(4,128)S(1)} %pad_maximum_fusion.1), channel_id=1, replica_groups=mesh['rep'=8,'fs'=2,'tp'=2] {'rep'}, use_global_device_ids=true, to_apply=%region_7.8 | all-reduce | flops 4224 | bytes 33792 | tf_op jit(solution)/shard_map/psum | solution.py:85
  150.7 0.6 broadcast_multiply_fusion.3
  151.3 0.0 reduce-scatter.2.cloned.1.call-done
  151.3 2.1 convert_element_type.46
  153.4 272.0 %all-reduce.12.cloned.1.call-done = (f32[1024,704]{0,1:T(8,128)}, f32[1024,704]{0,1:T(8,128)}, f32[704,1024]{1,0:T(8,128)}) async-done(((f32[1024,704]{0,1:T(8,128)}, f32[1024,704]{0,1:T(8,128)}, f32[704,1024]{1,0:T(8,128)}), (f32[1024,704]{0,1:T(8,128)}, f32[1024,704]{0,1:T(8,128)}, f32[704,1024]{1,0:T(8,128)})) %all-reduce.12.cloned.1.call-update) | async-done | bytes 8650768 | tf_op jit(solution)/shard_map/psum | solution.py:85
  425.4 4.1 broadcast_multiply_fusion.2
  429.5 0.0 copy-done.3
  429.5 1.9 broadcast_multiply_fusion.1
  431.4 1.0 copy-done.2
  432.4 1.9 broadcast_multiply_fusion
  434.3 0.0 copy-done.1
  (11 shorter events, 0.1 us)
Async XLA Ops:
  7.2 51.9 %copy-start = (bf16[704,1024]{1,0:T(8,128)(2,1)S(1)}, bf16[704,1024]{1,0:T(8,128)(2,1)}, u32[]{:S(2)}) copy-start(bf16[704,1024]{1,0:T(8,128)(2,1)} %param.11) | copy-start | bytes 4325380
  7.2 27.7 %all-gather.5.cloned.1.call-start = ((), (), s32[]{:S(2)}) async-start(), calls=%async_computation.2 | async-start | bytes 2621440 | tf_op jit(solution)/shard_map/all_gather | solution.py:54
  7.9 51.1 %all-gather.3.cloned.1.call-start = ((), (), s32[]{:S(2)}) async-start(), calls=%async_computation.1 | async-start | bytes 2621440 | tf_op jit(solution)/shard_map/all_gather | solution.py:59
  8.7 142.6 %reduce-scatter.2.cloned.1.call-start = ((), (), s32[]{:S(2)}) async-start(), calls=%async_computation.3 | async-start | bytes 5242880 | tf_op jit(solution)/shard_map/reduce_scatter | solution.py:74
  40.5 1.6 copy-start.4
  82.7 11.0 %copy-start.7 = (bf16[1024,704]{0,1:T(8,128)(2,1)S(1)}, bf16[1024,704]{0,1:T(8,128)(2,1)}, u32[]{:S(2)}) copy-start(bf16[1024,704]{0,1:T(8,128)(2,1)} %param.9) | copy-start | bytes 4325380
  93.7 1.9 copy-start.8
  99.5 325.9 %all-reduce.12.cloned.1.call-start = ((), (), s32[]{:S(2)}) async-start(), calls=%async_computation.4 | async-start | bytes 17301504 | tf_op jit(solution)/shard_map/psum | solution.py:85
  99.7 5.0 %copy-start.5 = (bf16[1024,1024]{1,0:T(8,128)(2,1)S(1)}, bf16[1024,1024]{1,0:T(8,128)(2,1)}, u32[]{:S(2)}) copy-start(bf16[1024,1024]{1,0:T(8,128)(2,1)} %all-gather.5.cloned.1.call-done) | copy-start | bytes 6291460
  104.7 3.4 copy-start.6
  104.7 3.4 copy-start.9
  104.7 5.0 %copy-start.10 = (f32[1024,704]{0,1:T(8,128)S(1)}, f32[1024,704]{0,1:T(8,128)}, u32[]{:S(2)}) copy-start(f32[1024,704]{0,1:T(8,128)} %get-tuple-element.30) | copy-start | bytes 8650756
  425.4 4.1 copy-start.3
  429.5 2.9 copy-start.2
  431.4 2.9 copy-start.1
Sparse Core Ops, SparseCore 0:
  9.5 25.2 all-gather.4
  36.4 22.5 all-gather.2
  99.6 44.5 reduce-scatter.1
  149.0 276.3 all-reduce.11
where the time goes:
time: 441 us
  waiting for transfers between devices  312 us (71%)
  matrix products  46.6 us (11%)
  blocking collectives  37.6 us (9%)
  other arithmetic  24.9 us (6%)
  between operations  13.9 us (3%)
  local copies, waits for them, and re-layouts  5.95 us (1%)
    psum x1, waiting for transfers between devices, per_device(): lax.psum((gate_part, value_part, down_part, gate_tap_part, value_tap_part...  272 us
    psum x1, blocking collectives, per_device(): lax.psum((gate_part, value_part, down_part, gate_tap_part, value_tap_part...  37.6 us
    dot_general x3, matrix products, contract_cols(): lax.dot_general(left, right, (((1,), (1,)), ((), ())), preferred_element_...  29.3 us
    all_gather x1, waiting for transfers between devices, per_device(): piece = lax.all_gather(tokens, ('fs', 'tp'), axis=0, tiled=True)  24.5 us
    all_gather x1, waiting for transfers between devices, per_device(): piece = lax.all_gather(cotangent, ('fs', 'tp'), axis=0, tiled=True)  13.7 us
    dot_general x3, matrix products, contract_rows(): lax.dot_general(left, right, (((0,), (0,)), ((), ())), preferred_element_...  11.6 us
    convert_element_type x1, other arithmetic, per_device(): grad_gate = reverse_mix(back_gate, gate_taps).astype(jnp.bfloat16)  11 us
  transfers between devices with their start and end apart: 4, of which 3 were waited for; matrix products, arithmetic and copies ran while one was open for 6% of the time, Pallas kernels for 0%

commit v1 on v0

v1 whole, which is shorter than its diff:
```python
import functools
import math

import jax
import jax.numpy as jnp
from jax import lax
from jax.experimental import pallas as pl
from jax.experimental.pallas import tpu as pltpu
from jax.sharding import PartitionSpec as P


F32 = jnp.float32
BF16 = jnp.bfloat16
LANES = 128
SUBLANES = 8
CHUNKS = 4
CALLS = 2
LIMIT = 60000 * 2**10
ORDERS = ((0, 1), (1, 0), (0, 1), (1, 0))
UNROLL = 1


def bit_count(size):
    return size.bit_length() - 1


def exchange(value, axis, bit):
    size = lax.axis_size(axis)
    return lax.ppermute(value, axis, [(i, i ^ (1 << bit)) for i in range(size)])


FINISH = (0, 1, 3, 2)


def rep_bit(bit):
    return (lax.axis_index("rep") >> bit) & 1


def dot_rows(left, right):
    return lax.dot_general(left, right, (((1,), (1,)), ((), ())), preferred_element_type=F32)


def dot(left, right):
    return lax.dot_general(left, right, (((1,), (0,)), ((), ())), preferred_element_type=F32)


def lane_index():
    return lax.broadcasted_iota(jnp.int32, (SUBLANES, LANES), 1)


def moved_later(tiles, offset):
    lane = lane_index()
    turned = [pltpu.roll(tile, offset, 1) for tile in tiles]
    before = [jnp.zeros_like(tiles[0])] + turned[:-1]
    return [jnp.where(lane < offset, b, t) for b, t in zip(before, turned)]


def moved_earlier(tiles, offset):
    lane = lane_index()
    turned = [pltpu.roll(tile, LANES - offset, 1) for tile in tiles]
    after = turned[1:] + [jnp.zeros_like(tiles[0])]
    return [jnp.where(lane >= LANES - offset, a, t) for a, t in zip(after, turned)]


def load_tiles(ref, at):
    return [ref[at, i : i + LANES] for i in range(0, ref.shape[1], LANES)]


def forward_kernel(parts, me_ref, *refs):
    pieces = refs[:parts]
    gate_ref, value_ref, gtaps_ref, vtaps_ref = refs[parts : parts + 4]
    hidden_ref, silu_ref, slope_ref, upg_ref, upv_ref = refs[parts + 4 :]
    height = gate_ref.shape[0]
    rows = pieces[0].shape[0]
    count = gtaps_ref.shape[1]
    weights = jnp.concatenate([gate_ref[...], value_ref[...]], axis=0)
    for r, piece in enumerate(pieces):
        at = pl.ds(pl.multiple_of((me_ref[0] ^ r) * rows, rows), rows)
        up = dot_rows(weights, piece[...]).astype(BF16)
        upg_ref[:, at] = up[:height]
        upv_ref[:, at] = up[height:]

    def mixed(tiles, taps_ref, at):
        total = None
        for k in range(count):
            tap = jnp.broadcast_to(taps_ref[at, k : k + 1], (SUBLANES, LANES))
            terms = [tap * tile for tile in (moved_later(tiles, k) if k else tiles)]
            total = terms if total is None else [a + b for a, b in zip(total, terms)]
        return total

    def body(i, carry):
        both = pl.ds(pl.multiple_of(i * 2 * SUBLANES, 2 * SUBLANES), 2 * SUBLANES)
        upg = [tile.astype(F32) for tile in load_tiles(upg_ref, both)]
        upv = [tile.astype(F32) for tile in load_tiles(upv_ref, both)]
        halves = []
        for half in range(2):
            rng = slice(half * SUBLANES, (half + 1) * SUBLANES)
            at = pl.ds(pl.multiple_of(i * 2 * SUBLANES + half * SUBLANES, SUBLANES), SUBLANES)
            gates = mixed([t[rng] for t in upg], gtaps_ref, at)
            values = mixed([t[rng] for t in upv], vtaps_ref, at)
            out = []
            for n, (gate, value) in enumerate(zip(gates, values)):
                sigma = jax.nn.sigmoid(gate)
                silu = gate * sigma
                lanes = slice(n * LANES, (n + 1) * LANES)
                silu_ref[at, lanes] = silu
                slope_ref[at, lanes] = value * sigma * (1.0 + gate * (1.0 - sigma))
                out.append(silu * value)
            halves.append(out)
        for n, (top, low) in enumerate(zip(*halves)):
            hidden_ref[both, n * LANES : (n + 1) * LANES] = jnp.concatenate([top, low], axis=0).astype(BF16)
        return carry

    lax.fori_loop(0, height // (2 * SUBLANES), body, 0, unroll=UNROLL)


def forward_part(me, pieces, gate_t, value_t, gtaps, vtaps):
    hidden, model = gate_t.shape
    parts, rows = len(pieces), pieces[0].shape[0]
    tokens, count = parts * rows, gtaps.shape[1]
    height = hidden // CHUNKS
    piece = pl.BlockSpec((rows, model), lambda i, me_ref: (0, 0))
    weight = pl.BlockSpec((height, model), lambda i, me_ref: (i, 0))
    taps = pl.BlockSpec((height, count), lambda i, me_ref: (i, 0))
    out = pl.BlockSpec((height, tokens), lambda i, me_ref: (i, 0))
    return pl.pallas_call(
        functools.partial(forward_kernel, parts),
        out_shape=tuple(jax.ShapeDtypeStruct((hidden, tokens), t) for t in (BF16, F32, F32, BF16, BF16)),
        grid_spec=pltpu.PrefetchScalarGridSpec(
            num_scalar_prefetch=1,
            grid=(CHUNKS,),
            in_specs=[piece] * parts + [weight, weight, taps, taps],
            out_specs=(out,) * 5,
        ),
        compiler_params=pltpu.CompilerParams(dimension_semantics=("arbitrary",), vmem_limit_bytes=LIMIT),
        cost_estimate=pl.CostEstimate(
            flops=4 * hidden * tokens * model, bytes_accessed=18 * hidden * tokens, transcendentals=2 * hidden * tokens
        ),
        name="forward_part",
    )(me, *pieces, gate_t, value_t, gtaps, vtaps)


def backward_kernel(parts, orders, call, me_ref, *refs):
    refs = list(refs)

    def take(count):
        taken, refs[:count] = refs[:count], []
        return taken

    subs = len(orders)
    sources = take(2 * parts + 6)
    gtaps_ref, vtaps_ref = take(2)
    targets = take(2 * subs + 2)
    (sums_ref,) = take(1)
    toks, cots, bufs = take(parts), take(parts), take(6)
    down_ref, hidden_ref, silu_ref, slope_ref, upg_ref, upv_ref = bufs
    outs, (ggrad_ref, vgrad_ref), (back, acc, in_sems, out_sems) = take(2 * subs), take(2), take(4)
    height, rows = down_ref.shape[0], toks[0].shape[0]
    count = gtaps_ref.shape[1]

    here = toks + cots + bufs
    mine = pl.ds(call * height, height)
    arrivals = [
        pltpu.make_async_copy(src if n < 2 * parts else src.at[mine], dst, in_sems.at[n])
        for n, (src, dst) in enumerate(zip(sources, here))
    ]
    order = [2 * parts, *range(parts, 2 * parts), *range(2 * parts + 2, 2 * parts + 6), 2 * parts + 1, *range(parts)]
    for n in order:
        arrivals[n].start()
    leaving = []

    def leave(src, dst):
        copy = pltpu.make_async_copy(src, dst, out_sems.at[len(leaving)])
        copy.start()
        leaving.append(copy)

    spots = [pl.ds(pl.multiple_of((me_ref[0] ^ r) * rows, rows), rows) for r in range(parts)]
    arrivals[2 * parts].wait()
    for r, (at, piece) in enumerate(zip(spots, cots)):
        arrivals[parts + r].wait()
        back[:, at] = dot_rows(down_ref[...], piece[...])
    for n in range(2 * parts + 2, 2 * parts + 6):
        arrivals[n].wait()

    def mixed(tiles, fields, taps_ref, at, first):
        total = None
        for k in range(count):
            tap = jnp.broadcast_to(taps_ref[at, k : k + 1], (SUBLANES, LANES))
            moved = moved_earlier(tiles, k) if k else tiles
            terms = [tap * tile for tile in moved]
            total = terms if total is None else [a + b for a, b in zip(total, terms)]
            acc[first + k, at] = sum(m * f for m, f in zip(moved, fields))
        return total

    def body(i, carry):
        both = pl.ds(pl.multiple_of(i * 2 * SUBLANES, 2 * SUBLANES), 2 * SUBLANES)
        upg = [tile.astype(F32) for tile in load_tiles(upg_ref, both)]
        upv = [tile.astype(F32) for tile in load_tiles(upv_ref, both)]
        gates, values = [], []
        for half in range(2):
            rng = slice(half * SUBLANES, (half + 1) * SUBLANES)
            at = pl.ds(pl.multiple_of(i * 2 * SUBLANES + half * SUBLANES, SUBLANES), SUBLANES)
            up = load_tiles(back, at)
            gback = [a * b for a, b in zip(up, load_tiles(slope_ref, at))]
            gates.append(mixed(gback, [t[rng] for t in upg], gtaps_ref, at, 0))
            vback = [a * b for a, b in zip(up, load_tiles(silu_ref, at))]
            values.append(mixed(vback, [t[rng] for t in upv], vtaps_ref, at, count))
        for ref, halves in ((ggrad_ref, gates), (vgrad_ref, values)):
            for n, (top, low) in enumerate(zip(*halves)):
                ref[both, n * LANES : (n + 1) * LANES] = jnp.concatenate([top, low], axis=0).astype(BF16)
        return carry

    lax.fori_loop(0, height // (2 * SUBLANES), body, 0, unroll=UNROLL)
    leave(ggrad_ref, targets[2 * subs])
    leave(vgrad_ref, targets[2 * subs + 1])
    for n in [2 * parts + 1, *range(parts)]:
        arrivals[n].wait()

    part = height // subs
    size = outs[0].shape[2]
    for pair in (3, 2, 1, 0):
        bits = (pair >> 1, pair & 1)
        cols = pl.ds(pl.multiple_of((me_ref[1] ^ pair) * size, size), size)
        both, down = None, None
        for at, tok, cot in zip(spots, toks, cots):
            term = dot(jnp.concatenate([ggrad_ref[:, at], vgrad_ref[:, at]], axis=0), tok[:, cols])
            both = term if both is None else both + term
            term = dot(hidden_ref[:, at], cot[:, cols])
            down = term if down is None else down + term
        both, down = both.astype(BF16), down.astype(BF16)
        for sub, (first, second) in enumerate(orders):
            which, spot = 2 * sub + 1 - bits[first], bits[second]
            ref, own = outs[which], slice(sub * part, (sub + 1) * part)
            ref[spot, :part] = both[own]
            ref[spot, part : 2 * part] = both[height:][own]
            ref[spot, 2 * part :] = down[own]
            leave(ref.at[spot], targets[which].at[spot])
    for k in range(2 * count):
        sums_ref[:, k : k + 1] = jnp.sum(acc[k], axis=1, keepdims=True)
    for copy in leaving:
        copy.wait()


def backward_part(call, me, toks, cots, down, hidden, silu, slope, upg, upv, gtaps, vtaps):
    full, model = down.shape
    parts, rows = len(toks), toks[0].shape[0]
    tokens, count = parts * rows, gtaps.shape[1]
    height, subs = full // CALLS, CHUNKS // CALLS

    def whole(shape):
        return pl.BlockSpec(shape, lambda i, me_ref: (0,) * len(shape))

    taps = pl.BlockSpec((height, count), lambda i, me_ref: (call, 0))
    payload = (2, 3 * height // subs, model // 4)
    anywhere = pl.BlockSpec(memory_space=pl.ANY)
    shapes = (payload,) * (2 * subs) + ((height, tokens), (height, tokens), (height, 2 * count))
    types = (BF16,) * (2 * subs + 2) + (F32,)
    return pl.pallas_call(
        functools.partial(backward_kernel, parts, ORDERS[call * subs : (call + 1) * subs], call),
        out_shape=tuple(jax.ShapeDtypeStruct(s, t) for s, t in zip(shapes, types)),
        grid_spec=pltpu.PrefetchScalarGridSpec(
            num_scalar_prefetch=1,
            grid=(1,),
            in_specs=[anywhere] * (2 * parts + 6) + [taps, taps],
            out_specs=(anywhere,) * (2 * subs + 2) + (whole(shapes[-1]),),
            scratch_shapes=[
                *[pltpu.VMEM((rows, model), BF16)] * (2 * parts),
                pltpu.VMEM((height, model), BF16),
                *[pltpu.VMEM((height, tokens), t) for t in (BF16, F32, F32, BF16, BF16)],
                *[pltpu.VMEM(payload, BF16)] * (2 * subs),
                *[pltpu.VMEM((height, tokens), BF16)] * 2,
                pltpu.VMEM((height, tokens), F32),
                pltpu.VMEM((2 * count, height, LANES), F32),
                pltpu.SemaphoreType.DMA((2 * parts + 6,)),
                pltpu.SemaphoreType.DMA((4 * subs + 2,)),
            ],
        ),
        compiler_params=pltpu.CompilerParams(dimension_semantics=("arbitrary",), vmem_limit_bytes=LIMIT),
        cost_estimate=pl.CostEstimate(
            flops=8 * height * tokens * model, bytes_accessed=8 * tokens * model, transcendentals=0
        ),
        name="backward_part",
    )(me, *toks, *cots, down, hidden, silu, slope, upg, upv, gtaps, vtaps)


def input_kernel(me_ref, *refs):
    count = (len(refs) - 4) // 2
    ggrads, vgrads = refs[:count], refs[count : 2 * count]
    gate_ref, value_ref, sent_ref, kept_ref = refs[2 * count :]
    height = ggrads[0].shape[0]
    total = None
    for grads, weight_ref in ((ggrads, gate_ref), (vgrads, value_ref)):
        for h, ref in enumerate(grads):
            term = lax.dot_general(
                ref[...], weight_ref[h * height : (h + 1) * height], (((0,), (0,)), ((), ())), preferred_element_type=F32
            )
            total = term if total is None else total + term
    step = pl.program_id(0)

    @pl.when(step < pl.num_programs(0) // 2)
    def _():
        sent_ref[0] = total.astype(BF16)

    @pl.when(step >= pl.num_programs(0) // 2)
    def _():
        kept_ref[0] = total


def input_part(me, ggrads, vgrads, gate_t, value_t, parts):
    hidden, model = gate_t.shape
    height, tokens = ggrads[0].shape
    rows, half = tokens // parts, parts // 2

    def relative(i):
        return jnp.where(i < half, 2 * i + 1, 2 * (i - half))

    field = pl.BlockSpec((height, rows), lambda i, me_ref: (0, me_ref[0] ^ relative(i)))
    weight = pl.BlockSpec((hidden, model), lambda i, me_ref: (0, 0))
    return pl.pallas_call(
        input_kernel,
        out_shape=(
            jax.ShapeDtypeStruct((half, rows, model), BF16),
            jax.ShapeDtypeStruct((half, rows, model), F32),
        ),
        grid_spec=pltpu.PrefetchScalarGridSpec(
            num_scalar_prefetch=1,
            grid=(parts,),
            in_specs=[field] * (2 * len(ggrads)) + [weight, weight],
            out_specs=(
                pl.BlockSpec((1, rows, model), lambda i, me_ref: (jnp.minimum(i, half - 1), 0, 0)),
                pl.BlockSpec((1, rows, model), lambda i, me_ref: (jnp.maximum(i - half, 0), 0, 0)),
            ),
        ),
        compiler_params=pltpu.CompilerParams(dimension_semantics=("arbitrary",), vmem_limit_bytes=LIMIT),
        cost_estimate=pl.CostEstimate(
            flops=4 * hidden * tokens * model, bytes_accessed=4 * hidden * tokens + 6 * tokens * model, transcendentals=0
        ),
        name="input_part",
    )(me, *ggrads, *vgrads, gate_t, value_t)


def add(left, right, dtype):
    return (left.astype(F32) + right.astype(F32)).astype(dtype)


def reduce_chunk(sent, kept, first, second):
    got = exchange(sent, "rep", first)
    over = exchange(add(kept[1], got[1], BF16), "rep", second)
    mine = add(add(kept[0], got[0], F32), over, BF16)
    rest = [b for b in range(bit_count(lax.axis_size("rep"))) if b not in (first, second)]
    for at, bit in enumerate(rest):
        mine = add(mine, exchange(mine, "rep", bit), BF16 if at == len(rest) - 1 else F32)
    pair = jnp.stack([mine, exchange(mine, "rep", second)])
    return pair, exchange(pair, "rep", first)


def place_kernel(scale, where_ref, near_ref, far_ref, *refs):
    outs = refs[-3:]
    height = outs[0].shape[0]
    step = pl.program_id(0)
    for near, ref in ((True, near_ref), (False, far_ref)):

        @pl.when((step < 2) == near)
        def _(ref=ref):
            for n, out_ref in enumerate(outs):
                out_ref[...] = ref[0, n * height : (n + 1) * height].astype(F32) * scale


def place(chunk, where, near, far, outs, shape, scale):
    swap = ORDERS[chunk][0] == 1
    hidden, model = shape
    height, size = hidden // CHUNKS, model // 4
    block = (1, *near.shape[1:])
    first = pl.BlockSpec(block, lambda i, where_ref: (jnp.minimum(i, 1), 0, 0))
    last = pl.BlockSpec(block, lambda i, where_ref: (jnp.maximum(i - 2, 0), 0, 0))

    def spot(i, where_ref):
        return chunk, ((i >> 1) | ((i & 1) << 1) if swap else i) ^ where_ref[1]

    spec = pl.BlockSpec((height, size), spot)
    return pl.pallas_call(
        functools.partial(place_kernel, scale),
        out_shape=(jax.ShapeDtypeStruct(shape, F32),) * 3,
        grid_spec=pltpu.PrefetchScalarGridSpec(
            num_scalar_prefetch=1,
            grid=(4,),
            in_specs=[first, last] + [pl.BlockSpec(memory_space=pl.ANY)] * len(outs),
            out_specs=(spec,) * 3,
        ),
        input_output_aliases={3 + n: n for n in range(len(outs))},
        compiler_params=pltpu.CompilerParams(dimension_semantics=("arbitrary",), vmem_limit_bytes=LIMIT),
        cost_estimate=pl.CostEstimate(flops=3 * height * model, bytes_accessed=18 * height * model, transcendentals=0),
        name="place",
    )(where, near, far, *outs)


def butterfly(value):
    for bit in range(bit_count(lax.axis_size("rep"))):
        value = value + exchange(value, "rep", bit)
    return value


def gather_relative(own):
    found = {0: own}
    base = bit_count(lax.axis_size("tp"))
    for bit in range(bit_count(lax.axis_size("fs"))):
        found.update({r | (1 << (base + bit)): exchange(item, "fs", bit) for r, item in list(found.items())})
    for bit in range(base):
        found.update({r | (1 << bit): exchange(item, "tp", bit) for r, item in list(found.items())})
    return [found[r] for r in range(len(found))]


def scatter_relative(sent, kept):
    moved = exchange(sent, "tp", 0)
    blocks = [add(kept[i], moved[i], F32) for i in range(kept.shape[0])]
    bits = [("tp", b) for b in range(1, bit_count(lax.axis_size("tp")))]
    bits += [("fs", b) for b in range(bit_count(lax.axis_size("fs")))]
    for axis, bit in bits:
        far = jnp.stack(blocks[1::2]).astype(BF16)
        moved = exchange(far, axis, bit)
        blocks = [add(item, moved[i], F32) for i, item in enumerate(blocks[0::2])]
    return blocks[0].astype(BF16)


def layer(tokens, cotangent, gate_weight, value_weight, down_weight, gate_taps, value_taps):
    rows, model = tokens.shape
    hidden = gate_weight.shape[1]
    parts = lax.axis_size("fs") * lax.axis_size("tp")
    scale = 1.0 / math.sqrt(rows * parts * lax.axis_size("rep"))
    me = (lax.axis_index("fs") * lax.axis_size("tp") + lax.axis_index("tp")).astype(jnp.int32)
    gate_t, value_t = gate_weight.T, value_weight.T
    gtaps, vtaps = gate_taps.T, value_taps.T
    where = jnp.stack([me, (2 * rep_bit(0) + rep_bit(1)).astype(jnp.int32)])

    cotangent, where, gtaps, vtaps = lax.optimization_barrier((cotangent, where, gtaps, vtaps))
    toks = gather_relative(tokens)
    cots = gather_relative(cotangent)
    fields = forward_part(where, toks, gate_t, value_t, gtaps, vtaps)
    ggrads, vgrads, sums, done = [], [], [], {}
    subs = CHUNKS // CALLS
    for call in range(CALLS):
        *payload, ggrad, vgrad, tapsum = backward_part(
            call, where, toks, cots, down_weight, *fields, gtaps, vtaps
        )
        for sub in range(subs):
            chunk = call * subs + sub
            done[chunk] = reduce_chunk(payload[2 * sub], payload[2 * sub + 1], *ORDERS[chunk])
        ggrads.append(ggrad)
        vgrads.append(vgrad)
        sums.append(tapsum)
    outs = ()
    for chunk in FINISH:
        outs = place(chunk, where, *done[chunk], outs, (hidden, model), scale)
    sums = butterfly(jnp.concatenate(sums, axis=0).T) * scale
    partial = input_part(where, ggrads, vgrads, gate_t, value_t, parts)
    input_grad = scatter_relative(*partial)
    count = gate_taps.shape[0]
    return input_grad, outs[0].T, outs[1].T, outs[2], sums[:count], sums[count:]


def solution(mesh):
    in_specs = (
        P(("rep", "fs", "tp"), None),
        P(("rep", "fs", "tp"), None),
        P(None, ("fs", "tp")),
        P(None, ("fs", "tp")),
        P(("fs", "tp"), None),
        P(None, ("fs", "tp")),
        P(None, ("fs", "tp")),
    )
    out_specs = (
        P(("rep", "fs", "tp"), None),
        P(None, ("fs", "tp")),
        P(None, ("fs", "tp")),
        P(("fs", "tp"), None),
        P(None, ("fs", "tp")),
        P(None, ("fs", "tp")),
    )
    return jax.shard_map(layer, mesh=mesh, in_specs=in_specs, out_specs=out_specs, check_vma=False)
```

time: 441 us -> 216 us (0.49)
  waiting for transfers between devices: 312 us -> 101 us
  Pallas kernels: 0 us -> 67.9 us
  matrix products: 46.6 us -> 0 us
  blocking collectives: 37.6 us -> 0 us
  starting transfers between devices: 0.34 us -> 31.9 us
  other arithmetic: 24.9 us -> 3.15 us
  between operations: 13.9 us -> 0.93 us
  local copies, waits for them, and re-layouts: 5.95 us -> 11.1 us
    psum x1 -> x0, waiting for transfers between devices: 272 us -> none  [per_device(): lax.psum((gate_part, value_part, down_part, gate_tap_part, value_tap_part...]
    ppermute x0 -> x31, waiting for transfers between devices: none -> 101 us  [exchange(): return lax.ppermute(value, axis, [(i, i ^ 1 << bit) for i in range(size)])]
    pallas_call x0 -> x8, Pallas kernels: none -> 67.9 us  [the longest x2 26.1 us: backward_part(): pl.pallas_call(functools.partial(backward_kernel, parts, ORDERS[call * su...]
    dot_general x7 -> x0, matrix products: 46.6 us -> none  [the longest x3 29.3 us: contract_cols(): lax.dot_general(left, right, (((1,), (1,)), ((), ())), preferred_element_...]
    all_gather x2 -> x0, waiting for transfers between devices: 38.1 us -> none  [the longest x1 24.5 us: per_device(): piece = lax.all_gather(tokens, ('fs', 'tp'), axis=0, tiled=True)]
    psum x1 -> x0, blocking collectives: 37.6 us -> none  [per_device(): lax.psum((gate_part, value_part, down_part, gate_tap_part, value_tap_part...]
    ppermute x0 -> x31, starting transfers between devices: none -> 31.9 us  [exchange(): return lax.ppermute(value, axis, [(i, i ^ 1 << bit) for i in range(size)])]
    convert_element_type x3 -> x14, other arithmetic: 16.3 us -> 2.16 us  [the longest x1 1.03 us: scatter_relative(): return blocks[0].astype(BF16)]
  transfers between devices with their start and end apart: 4 -> 31, of which waited for: 3 -> 17; matrix products, arithmetic and copies ran while one was open for 6% -> 3% of each run, Pallas kernels for 0% -> 17%
where the time goes in v1:
time: 216 us
  waiting for transfers between devices  101 us (47%)
  Pallas kernels  67.9 us (31%)
  starting transfers between devices  31.9 us (15%)
  local copies, waits for them, and re-layouts  11.1 us (5%)
  other arithmetic  3.15 us (1%)
    ppermute x31, waiting for transfers between devices, exchange(): return lax.ppermute(value, axis, [(i, i ^ 1 << bit) for i in range(size)])  101 us
    ppermute x31, starting transfers between devices, exchange(): return lax.ppermute(value, axis, [(i, i ^ 1 << bit) for i in range(size)])  31.9 us
    pallas_call x2, Pallas kernels, backward_part(): pl.pallas_call(functools.partial(backward_kernel, parts, ORDERS[call * su...  26.1 us
    pallas_call x4, Pallas kernels, place(): pl.pallas_call(functools.partial(place_kernel, scale), out_shape=(jax.Sha...  17.6 us
    pallas_call x1, Pallas kernels, forward_part(): pl.pallas_call(functools.partial(forward_kernel, parts), out_shape=tuple(...  14.5 us
    pallas_call x1, Pallas kernels, input_part(): pl.pallas_call(input_kernel, out_shape=(jax.ShapeDtypeStruct((half, rows,...  9.79 us
    unnamed x44, local copies, waits for them, and re-layouts  8.51 us
  transfers between devices with their start and end apart: 31, of which 17 were waited for; matrix products, arithmetic and copies ran while one was open for 3% of the time, Pallas kernels for 17%

profile of v1, /device:TPU:0, one launch (start us, length us, event | category | flops | bytes accessed | tf_op | source)
XLA Modules:
  0.0 215.5 jit_solution(10959061195719260758)
XLA Ops:
  0.6 3.0 %collective-permute-start.1 = (bf16[256,1024]{1,0:T(8,128)(2,1)}, bf16[256,1024]{1,0:T(8,128)(2,1)S(1)}, u32[]{:S(2)}, u32[]{:S(2)}) collective-permute-start(bf16[256,1024]{1,0:T(8,128)(2,1)} %refs_0_.5), channel_id=1, source_target_pairs={{0,2},{2,0},{1,3},{3,1},{4,6},{6,4},{5,7},{7,5},{8,10},{10,8},{9,1... | collective-permute-start | bytes 1572872 | tf_op jit(solution)/shard_map/ppermute | solution.py:29
  3.7 1.6 copy.26
  5.3 1.6 copy.27
  7.6 9.1 %collective-permute-done.1.refs_2_ = bf16[256,1024]{1,0:T(8,128)(2,1)S(1)} collective-permute-done((bf16[256,1024]{1,0:T(8,128)(2,1)}, bf16[256,1024]{1,0:T(8,128)(2,1)S(1)}, u32[]{:S(2)}, u32[]{:S(2)}) %collective-permute-start.1) | collective-permute-done | bytes 524320 | tf_op jit(solution)/shard_map/ppermute | solution.py:29
  17.2 9.9 %collective-permute-done.4.refs_6_ = bf16[256,1024]{1,0:T(8,128)(2,1)S(1)} collective-permute-done((bf16[256,1024]{1,0:T(8,128)(2,1)}, bf16[256,1024]{1,0:T(8,128)(2,1)S(1)}, u32[]{:S(2)}, u32[]{:S(2)}) %collective-permute-start.4) | collective-permute-done | bytes 524320 | tf_op jit(solution)/shard_map/ppermute | solution.py:29
  27.1 0.8 copy-done.6
  28.1 14.5 %forward_part.1 = (bf16[704,1024]{1,0:T(8,128)(2,1)}, f32[704,1024]{1,0:T(8,128)}, f32[704,1024]{1,0:T(8,128)}, bf16[704,1024]{1,0:T(8,128)(2,1)}, bf16[704,1024]{1,0:T(8,128)(2,1)}) custom-call(s32[2]{0:T(128)} %pad_add_fusion.me_ref.where_ref, bf16[256,1024]{1,0:T(8,128)(2,1)} %refs_0_.5, bf16[256,1024]{1,0:T(8,128)(2,1)} %copy-done.6, ...), custom_call_target="tpu_custom_call" | custom-call | flops 2952790016 | bytes 12976128 | tf_op jit(solution)/shard_map/forward_part/pallas_call | solution.py:126
  43.6 12.9 %backward_part.3 = (bf16[2,528,256]{2,1,0:T(8,128)(2,1)}, bf16[2,528,256]{2,1,0:T(8,128)(2,1)}, bf16[2,528,256]{2,1,0:T(8,128)(2,1)}, bf16[2,528,256]{2,1,0:T(8,...) custom-call(s32[2]{0:T(128)} %pad_add_fusion.me_ref.where_ref, ...), custom_call_target="tpu_custom_call" | custom-call | flops 2952790016 | bytes 8388608 | tf_op jit(solution)/shard_map/backward_part/pallas_call | solution.py:258
  56.6 1.0 copy.29
  57.6 13.1 %backward_part.2 = (bf16[2,528,256]{2,1,0:T(8,128)(2,1)}, bf16[2,528,256]{2,1,0:T(8,128)(2,1)}, bf16[2,528,256]{2,1,0:T(8,128)(2,1)}, bf16[2,528,256]{2,1,0:T(8,...) custom-call(s32[2]{0:T(128)} %pad_add_fusion.me_ref.where_ref, ...), custom_call_target="tpu_custom_call" | custom-call | flops 2952790016 | bytes 8388608 | tf_op jit(solution)/shard_map/backward_part/pallas_call | solution.py:258
  70.7 1.0 copy.28
  71.7 1.8 collective-permute-start.8
  73.9 1.8 collective-permute-start.13
  75.9 1.8 collective-permute-start.23
  77.7 9.8 %collective-permute-done.28 = f32[6,704]{1,0:T(8,128)S(1)} collective-permute-done((f32[6,704]{1,0:T(8,128)S(1)}, f32[6,704]{1,0:T(8,128)S(1)}, u32[]{:S(2)}, u32[]{:S(2)}) %collective-permute-start.28) | collective-permute-done | bytes 16928 | tf_op jit(solution)/shard_map/ppermute | solution.py:29
  87.6 1.8 collective-permute-start.29
  89.4 9.8 %input_part.1 = (bf16[2,256,1024]{2,1,0:T(8,128)(2,1)}, f32[2,256,1024]{2,1,0:T(8,128)}) custom-call(s32[2]{0:T(128)} %pad_add_fusion.me_ref.where_ref, bf16[352,1024]{1,0:T(8,128)(2,1)} %get-tuple-element.52.refs_0_, bf16[352,1024]{1,0:T(8,128)(2,1)} %get-tuple-element.53.refs_1_, bf16[352,1024]{1,0:T(8,128)(2,1)} %get-tuple-element.54.refs_2_, ...), custom_call_target="tpu_custom_call" | custom-call | flops 2952790016 | bytes 9175040 | tf_op jit(solution)/shard_map/input_part/pallas_call | solution.py:319
  99.2 1.0 collective-permute-done.29
  100.2 2.8 %collective-permute-start.30 = (f32[6,704]{1,0:T(8,128)S(1)}, f32[6,704]{1,0:T(8,128)S(1)}, u32[]{:S(2)}, u32[]{:S(2)}) collective-permute-start(f32[6,704]{1,0:T(8,128)S(1)} %add.117), channel_id=1, source_target_pairs={{0,16},{4,20},{8,24},{12,28},{16,0},{20,4},{24,8},{28,12},{1,17},{... | collective-permute-start | bytes 50696 | tf_op jit(solution)/shard_map/ppermute | solution.py:29
  103.1 1.6 collective-permute-start.9
  104.8 1.6 collective-permute-start.14
  107.1 4.6 %collective-permute-done.9 = bf16[528,256]{1,0:T(8,128)(2,1)S(1)} collective-permute-done((bf16[528,256]{1,0:T(8,128)(2,1)S(1)}, bf16[528,256]{1,0:T(8,128)(2,1)S(1)}, u32[]{:S(2)}, u32[]{:S(2)}) %collective-permute-start.9) | collective-permute-done | bytes 270368 | tf_op jit(solution)/shard_map/ppermute | solution.py:29
  111.8 1.6 collective-permute-start.24
  114.7 4.3 %collective-permute-done.19 = bf16[528,256]{1,0:T(8,128)(2,1)S(1)} collective-permute-done((bf16[528,256]{1,0:T(8,128)(2,1)S(1)}, bf16[528,256]{1,0:T(8,128)(2,1)S(1)}, u32[]{:S(2)}, u32[]{:S(2)}) %collective-permute-start.19) | collective-permute-done | bytes 270368 | tf_op jit(solution)/shard_map/ppermute | solution.py:29
  119.5 3.8 %collective-permute-done.24 = bf16[528,256]{1,0:T(8,128)(2,1)S(1)} collective-permute-done((bf16[528,256]{1,0:T(8,128)(2,1)S(1)}, bf16[528,256]{1,0:T(8,128)(2,1)S(1)}, u32[]{:S(2)}, u32[]{:S(2)}) %collective-permute-start.24) | collective-permute-done | bytes 270368 | tf_op jit(solution)/shard_map/ppermute | solution.py:29
  123.3 2.3 %collective-permute-start.20 = (bf16[528,256]{1,0:T(8,128)(2,1)S(1)}, bf16[528,256]{1,0:T(8,128)(2,1)S(1)}, u32[]{:S(2)}, u32[]{:S(2)}) collective-permute-start(bf16[528,256]{1,0:T(8,128)(2,1)S(1)} %fusion.1), channel_id=1, source_target_pairs={{0,16},{4,20},{8,24},{12,28},{16,0},{20,4},{24,8},{28,12},{1,17},{... | collective-permute-start | bytes 811016 | tf_op jit(solution)/shard_map/ppermute | solution.py:29
  126.5 20.6 %collective-permute-done.10 = bf16[528,256]{1,0:T(8,128)(2,1)S(1)} collective-permute-done((bf16[528,256]{1,0:T(8,128)(2,1)S(1)}, bf16[528,256]{1,0:T(8,128)(2,1)S(1)}, u32[]{:S(2)}, u32[]{:S(2)}) %collective-permute-start.10) | collective-permute-done | bytes 270368 | tf_op jit(solution)/shard_map/ppermute | solution.py:29
  147.2 1.5 collective-permute-start.7
  148.7 4.3 %collective-permute-done.15 = bf16[528,256]{1,0:T(8,128)(2,1)S(1)} collective-permute-done((bf16[528,256]{1,0:T(8,128)(2,1)S(1)}, bf16[528,256]{1,0:T(8,128)(2,1)S(1)}, u32[]{:S(2)}, u32[]{:S(2)}) %collective-permute-start.15) | collective-permute-done | bytes 270368 | tf_op jit(solution)/shard_map/ppermute | solution.py:29
  153.1 5.7 %collective-permute-done.20 = bf16[528,256]{1,0:T(8,128)(2,1)S(1)} collective-permute-done((bf16[528,256]{1,0:T(8,128)(2,1)S(1)}, bf16[528,256]{1,0:T(8,128)(2,1)S(1)}, u32[]{:S(2)}, u32[]{:S(2)}) %collective-permute-start.20) | collective-permute-done | bytes 270368 | tf_op jit(solution)/shard_map/ppermute | solution.py:29
  158.8 1.5 collective-permute-start.16
  160.4 2.2 %collective-permute-done.25 = bf16[528,256]{1,0:T(8,128)(2,1)S(1)} collective-permute-done((bf16[528,256]{1,0:T(8,128)(2,1)S(1)}, bf16[528,256]{1,0:T(8,128)(2,1)S(1)}, u32[]{:S(2)}, u32[]{:S(2)}) %collective-permute-start.25) | collective-permute-done | bytes 270368 | tf_op jit(solution)/shard_map/ppermute | solution.py:29
  162.6 1.5 collective-permute-start.21
  164.2 4.1 %collective-permute-done.11 = bf16[528,256]{1,0:T(8,128)(2,1)S(1)} collective-permute-done((bf16[528,256]{1,0:T(8,128)(2,1)S(1)}, bf16[528,256]{1,0:T(8,128)(2,1)S(1)}, u32[]{:S(2)}, u32[]{:S(2)}) %collective-permute-start.11) | collective-permute-done | bytes 270368 | tf_op jit(solution)/shard_map/ppermute | solution.py:29
  168.4 1.6 collective-permute-start.12
  170.0 1.1 collective-permute-done.21
  171.1 1.0 collective-permute-start.17
  172.2 5.5 %collective-permute-done.26 = bf16[528,256]{1,0:T(8,128)(2,1)S(1)} collective-permute-done((bf16[528,256]{1,0:T(8,128)(2,1)S(1)}, bf16[528,256]{1,0:T(8,128)(2,1)S(1)}, u32[]{:S(2)}, u32[]{:S(2)}) %collective-permute-start.26) | collective-permute-done | bytes 270368 | tf_op jit(solution)/shard_map/ppermute | solution.py:29
  177.7 1.6 collective-permute-start.27
  179.9 1.0 fusion.4
  181.0 13.3 %collective-permute-done.27.far_ref = bf16[2,528,256]{2,1,0:T(8,128)(2,1)S(1)} collective-permute-done((bf16[2,528,256]{2,1,0:T(8,128)(2,1)S(1)}, bf16[2,528,256]{2,1,0:T(8,128)(2,1)S(1)}, u32[]{:S(2)}, u32[]{:S(2)}) %collective-permute-start.27) | collective-permute-done | bytes 540704 | tf_op jit(solution)/shard_map/ppermute | solution.py:29
  195.1 4.4 %place.4 = (f32[704,1024]{1,0:T(8,128)}, f32[704,1024]{1,0:T(8,128)}, f32[704,1024]{1,0:T(8,128)}) custom-call(s32[2]{0:T(128)} %pad_add_fusion.me_ref.where_ref, bf16[2,528,256]{2,1,0:T(8,128)(2,1)} %copy-done.3, bf16[2,528,256]{2,1,0:T(8,128)(2,1)} %copy-done.18), custom_call_target="tpu_custom_call" | custom-call | flops 540672 | bytes 3244032 | tf_op jit(solution)/shard_map/place/pallas_call | solution.py:381
  199.9 0.8 copy-done.13
  200.7 4.4 %place.5 = (f32[704,1024]{1,0:T(8,128)}, f32[704,1024]{1,0:T(8,128)}, f32[704,1024]{1,0:T(8,128)}) custom-call(s32[2]{0:T(128)} %pad_add_fusion.me_ref.where_ref, bf16[2,528,256]{2,1,0:T(8,128)(2,1)} %copy-done.2, bf16[2,528,256]{2,1,0:T(8,128)(2,1)} %copy-done.13, ...), custom_call_target="tpu_custom_call", output_to_operand_aliasing={{0}: (3, {}), {1}: (4, {}), {2}: (5, {})} | custom-call | flops 540672 | bytes 3244032 | tf_op jit(solution)/shard_map/place/pallas_call | solution.py:381
  205.1 0.8 copy-done.12
  205.9 4.4 %place.6 = (f32[704,1024]{1,0:T(8,128)}, f32[704,1024]{1,0:T(8,128)}, f32[704,1024]{1,0:T(8,128)}) custom-call(s32[2]{0:T(128)} %pad_add_fusion.me_ref.where_ref, bf16[2,528,256]{2,1,0:T(8,128)(2,1)} %copy-done.1, bf16[2,528,256]{2,1,0:T(8,128)(2,1)} %copy-done.12, ...), custom_call_target="tpu_custom_call", output_to_operand_aliasing={{0}: (3, {}), {1}: (4, {}), {2}: (5, {})} | custom-call | flops 540672 | bytes 3244032 | tf_op jit(solution)/shard_map/place/pallas_call | solution.py:381
  210.3 0.8 copy-done.11
  211.1 4.4 %place.7 = (f32[704,1024]{1,0:T(8,128)}, f32[704,1024]{1,0:T(8,128)}, f32[704,1024]{1,0:T(8,128)}) custom-call(s32[2]{0:T(128)} %pad_add_fusion.me_ref.where_ref, bf16[2,528,256]{2,1,0:T(8,128)(2,1)} %copy-done, bf16[2,528,256]{2,1,0:T(8,128)(2,1)} %copy-done.11, ...), custom_call_target="tpu_custom_call", output_to_operand_aliasing={{0}: (3, {}), {1}: (4, {}), {2}: (5, {})} | custom-call | flops 540672 | bytes 3244032 | tf_op jit(solution)/shard_map/place/pallas_call | solution.py:381
  (92 shorter events, 8.9 us)
Async XLA Ops:
  0.6 16.0 %collective-permute-start.1 = (bf16[256,1024]{1,0:T(8,128)(2,1)}, bf16[256,1024]{1,0:T(8,128)(2,1)S(1)}, u32[]{:S(2)}, u32[]{:S(2)}) collective-permute-start(bf16[256,1024]{1,0:T(8,128)(2,1)} %refs_0_.5), channel_id=1, source_target_pairs={{0,2},{2,0},{1,3},{3,1},{4,6},{6,4},{5,7},{7,5},{8,10},{10,8},{9,1... | collective-permute-start | bytes 1572872 | tf_op jit(solution)/shard_map/ppermute | solution.py:29
  7.5 19.5 %collective-permute-start.4 = (bf16[256,1024]{1,0:T(8,128)(2,1)}, bf16[256,1024]{1,0:T(8,128)(2,1)S(1)}, u32[]{:S(2)}, u32[]{:S(2)}) collective-permute-start(bf16[256,1024]{1,0:T(8,128)(2,1)} %refs_4_.1), channel_id=1, source_target_pairs={{0,2},{2,0},{1,3},{3,1},{4,6},{6,4},{5,7},{7,5},{8,10},{10,8},{9,1... | collective-permute-start | bytes 1572872 | tf_op jit(solution)/shard_map/ppermute | solution.py:29
  7.6 19.5 %collective-permute-start = (bf16[256,1024]{1,0:T(8,128)(2,1)}, bf16[256,1024]{1,0:T(8,128)(2,1)S(1)}, u32[]{:S(2)}, u32[]{:S(2)}) collective-permute-start(bf16[256,1024]{1,0:T(8,128)(2,1)} %refs_0_.5), channel_id=1, source_target_pairs={{0,1},{1,0},{2,3},{3,2},{4,5},{5,4},{6,7},{7,6},{8,9},{9,8},{10,11... | collective-permute-start | bytes 1572872 | tf_op jit(solution)/shard_map/ppermute | solution.py:29
  16.6 10.4 %copy-start.4 = (bf16[256,1024]{1,0:T(8,128)(2,1)}, bf16[256,1024]{1,0:T(8,128)(2,1)S(1)}, u32[]{:S(2)}) copy-start(bf16[256,1024]{1,0:T(8,128)(2,1)S(1)} %collective-permute-done.1.refs_2_) | copy-start | bytes 1572868
  16.7 10.4 %collective-permute-start.2 = (bf16[256,1024]{1,0:T(8,128)(2,1)S(1)}, bf16[256,1024]{1,0:T(8,128)(2,1)S(1)}, u32[]{:S(2)}, u32[]{:S(2)}) collective-permute-start(bf16[256,1024]{1,0:T(8,128)(2,1)S(1)} %collective-permute-done.1.refs_2_), channel_id=1, source_target_pairs={{0,1},{1,0},{2,3},{3,2},{4,5},{5,4},{6,7},{7,6},{8,9},{9,8},{10,11... | collective-permute-start | bytes 1572872 | tf_op jit(solution)/shard_map/ppermute | solution.py:29
  16.7 26.0 %collective-permute-start.3 = (bf16[256,1024]{1,0:T(8,128)(2,1)}, bf16[256,1024]{1,0:T(8,128)(2,1)S(1)}, u32[]{:S(2)}, u32[]{:S(2)}) collective-permute-start(bf16[256,1024]{1,0:T(8,128)(2,1)} %refs_4_.1), channel_id=1, source_target_pairs={{0,1},{1,0},{2,3},{3,2},{4,5},{5,4},{6,7},{7,6},{8,9},{9,8},{10,11... | collective-permute-start | bytes 1572872 | tf_op jit(solution)/shard_map/ppermute | solution.py:29
  27.0 15.6 %copy-start.5 = (bf16[256,1024]{1,0:T(8,128)(2,1)}, bf16[256,1024]{1,0:T(8,128)(2,1)S(1)}, u32[]{:S(2)}) copy-start(bf16[256,1024]{1,0:T(8,128)(2,1)S(1)} %collective-permute-done.4.refs_6_) | copy-start | bytes 1572868
  27.0 15.6 %collective-permute-start.5 = (bf16[256,1024]{1,0:T(8,128)(2,1)S(1)}, bf16[256,1024]{1,0:T(8,128)(2,1)S(1)}, u32[]{:S(2)}, u32[]{:S(2)}) collective-permute-start(bf16[256,1024]{1,0:T(8,128)(2,1)S(1)} %collective-permute-done.4.refs_6_), channel_id=1, source_target_pairs={{0,1},{1,0},{2,3},{3,2},{4,5},{5,4},{6,7},{7,6},{8,9},{9,8},{10,11... | collective-permute-start | bytes 1572872 | tf_op jit(solution)/shard_map/ppermute | solution.py:29
  27.0 0.8 copy-start.6
  27.1 1.0 copy-start.7
  42.6 1.0 copy-start.9
  57.6 14.2 %copy-start.20 = (bf16[2,528,256]{2,1,0:T(8,128)(2,1)S(1)}, bf16[2,528,256]{2,1,0:T(8,128)(2,1)}, u32[]{:S(2)}) copy-start(bf16[2,528,256]{2,1,0:T(8,128)(2,1)} %get-tuple-element.59) | copy-start | bytes 1622020
  57.6 16.3 %copy-start.19 = (bf16[2,528,256]{2,1,0:T(8,128)(2,1)S(1)}, bf16[2,528,256]{2,1,0:T(8,128)(2,1)}, u32[]{:S(2)}) copy-start(bf16[2,528,256]{2,1,0:T(8,128)(2,1)} %get-tuple-element.61) | copy-start | bytes 1622020
  71.7 28.5 %collective-permute-start.8 = (bf16[2,528,256]{2,1,0:T(8,128)(2,1)S(1)}, bf16[2,528,256]{2,1,0:T(8,128)(2,1)S(1)}, u32[]{:S(2)}, u32[]{:S(2)}) collective-permute-start(bf16[2,528,256]{2,1,0:T(8,128)(2,1)S(1)} %copy-done.20), channel_id=1, source_target_pairs={{0,4},{4,0},{8,12},{12,8},{16,20},{20,16},{24,28},{28,24},{1,5},{5... | collective-permute-start | bytes 1622024 | tf_op jit(solution)/shard_map/ppermute | solution.py:29
  73.7 13.8 %collective-permute-start.28 = (f32[6,704]{1,0:T(8,128)S(1)}, f32[6,704]{1,0:T(8,128)S(1)}, u32[]{:S(2)}, u32[]{:S(2)}) collective-permute-start(f32[6,704]{1,0:T(8,128)S(1)} %maximum_bitcast_fusion), channel_id=1, source_target_pairs={{0,4},{4,0},{8,12},{12,8},{16,20},{20,16},{24,28},{28,24},{1,5},{5... | collective-permute-start | bytes 50696 | tf_op jit(solution)/shard_map/ppermute | solution.py:29
  73.9 29.2 %collective-permute-start.13 = (bf16[2,528,256]{2,1,0:T(8,128)(2,1)S(1)}, bf16[2,528,256]{2,1,0:T(8,128)(2,1)S(1)}, u32[]{:S(2)}, u32[]{:S(2)}) collective-permute-start(bf16[2,528,256]{2,1,0:T(8,128)(2,1)S(1)} %copy-done.19), channel_id=1, source_target_pairs={{0,8},{4,12},{8,0},{12,4},{16,24},{20,28},{24,16},{28,20},{1,9},{5... | collective-permute-start | bytes 1622024 | tf_op jit(solution)/shard_map/ppermute | solution.py:29
  75.7 29.1 %collective-permute-start.18 = (bf16[2,528,256]{2,1,0:T(8,128)(2,1)}, bf16[2,528,256]{2,1,0:T(8,128)(2,1)S(1)}, u32[]{:S(2)}, u32[]{:S(2)}) collective-permute-start(bf16[2,528,256]{2,1,0:T(8,128)(2,1)} %get-tuple-element.63), channel_id=1, source_target_pairs={{0,8},{4,12},{8,0},{12,4},{16,24},{20,28},{24,16},{28,20},{1,9},{5... | collective-permute-start | bytes 1622024 | tf_op jit(solution)/shard_map/ppermute | solution.py:29
  75.9 30.5 %collective-permute-start.23 = (bf16[2,528,256]{2,1,0:T(8,128)(2,1)}, bf16[2,528,256]{2,1,0:T(8,128)(2,1)S(1)}, u32[]{:S(2)}, u32[]{:S(2)}) collective-permute-start(bf16[2,528,256]{2,1,0:T(8,128)(2,1)} %get-tuple-element.65), channel_id=1, source_target_pairs={{0,4},{4,0},{8,12},{12,8},{16,20},{20,16},{24,28},{28,24},{1,5},{5... | collective-permute-start | bytes 1622024 | tf_op jit(solution)/shard_map/ppermute | solution.py:29
  87.6 12.6 %collective-permute-start.29 = (f32[6,704]{1,0:T(8,128)S(1)}, f32[6,704]{1,0:T(8,128)S(1)}, u32[]{:S(2)}, u32[]{:S(2)}) collective-permute-start(f32[6,704]{1,0:T(8,128)S(1)} %fusion.9), channel_id=1, source_target_pairs={{0,8},{4,12},{8,0},{12,4},{16,24},{20,28},{24,16},{28,20},{1,9},{5... | collective-permute-start | bytes 50696 | tf_op jit(solution)/shard_map/ppermute | solution.py:29
  89.4 13.6 %copy-start.17 = (bf16[2,528,256]{2,1,0:T(8,128)(2,1)S(1)}, bf16[2,528,256]{2,1,0:T(8,128)(2,1)}, u32[]{:S(2)}) copy-start(bf16[2,528,256]{2,1,0:T(8,128)(2,1)} %get-tuple-element.58) | copy-start | bytes 1622020
  89.4 15.4 %copy-start.16 = (bf16[2,528,256]{2,1,0:T(8,128)(2,1)S(1)}, bf16[2,528,256]{2,1,0:T(8,128)(2,1)}, u32[]{:S(2)}) copy-start(bf16[2,528,256]{2,1,0:T(8,128)(2,1)} %get-tuple-element.60) | copy-start | bytes 1622020
  89.4 17.0 %copy-start.15 = (bf16[2,528,256]{2,1,0:T(8,128)(2,1)S(1)}, bf16[2,528,256]{2,1,0:T(8,128)(2,1)}, u32[]{:S(2)}) copy-start(bf16[2,528,256]{2,1,0:T(8,128)(2,1)} %get-tuple-element.62) | copy-start | bytes 1622020
  89.4 17.7 %copy-start.14 = (bf16[2,528,256]{2,1,0:T(8,128)(2,1)S(1)}, bf16[2,528,256]{2,1,0:T(8,128)(2,1)}, u32[]{:S(2)}) copy-start(bf16[2,528,256]{2,1,0:T(8,128)(2,1)} %get-tuple-element.64) | copy-start | bytes 1622020
  100.2 25.5 %collective-permute-start.6 = (bf16[2,256,1024]{2,1,0:T(8,128)(2,1)}, bf16[2,256,1024]{2,1,0:T(8,128)(2,1)S(1)}, u32[]{:S(2)}, u32[]{:S(2)}) collective-permute-start(bf16[2,256,1024]{2,1,0:T(8,128)(2,1)} %get-tuple-element.57), channel_id=1, source_target_pairs={{0,1},{1,0},{2,3},{3,2},{4,5},{5,4},{6,7},{7,6},{8,9},{9,8},{10,11... | collective-permute-start | bytes 3145736 | tf_op jit(solution)/shard_map/ppermute | solution.py:29
  100.2 77.5 %collective-permute-start.30 = (f32[6,704]{1,0:T(8,128)S(1)}, f32[6,704]{1,0:T(8,128)S(1)}, u32[]{:S(2)}, u32[]{:S(2)}) collective-permute-start(f32[6,704]{1,0:T(8,128)S(1)} %add.117), channel_id=1, source_target_pairs={{0,16},{4,20},{8,24},{12,28},{16,0},{20,4},{24,8},{28,12},{1,17},{... | collective-permute-start | bytes 50696 | tf_op jit(solution)/shard_map/ppermute | solution.py:29
  103.1 8.7 %collective-permute-start.9 = (bf16[528,256]{1,0:T(8,128)(2,1)S(1)}, bf16[528,256]{1,0:T(8,128)(2,1)S(1)}, u32[]{:S(2)}, u32[]{:S(2)}) collective-permute-start(bf16[528,256]{1,0:T(8,128)(2,1)S(1)} %fusion.5), channel_id=1, source_target_pairs={{0,8},{4,12},{8,0},{12,4},{16,24},{20,28},{24,16},{28,20},{1,9},{5... | collective-permute-start | bytes 811016 | tf_op jit(solution)/shard_map/ppermute | solution.py:29
  104.8 9.4 %collective-permute-start.14 = (bf16[528,256]{1,0:T(8,128)(2,1)S(1)}, bf16[528,256]{1,0:T(8,128)(2,1)S(1)}, u32[]{:S(2)}, u32[]{:S(2)}) collective-permute-start(bf16[528,256]{1,0:T(8,128)(2,1)S(1)} %fusion.6), channel_id=1, source_target_pairs={{0,4},{4,0},{8,12},{12,8},{16,20},{20,16},{24,28},{28,24},{1,5},{5... | collective-permute-start | bytes 811016 | tf_op jit(solution)/shard_map/ppermute | solution.py:29
  106.4 20.0 %copy-start.10 = (f32[2,256,1024]{2,1,0:T(8,128)S(1)}, f32[2,256,1024]{2,1,0:T(8,128)}, u32[]{:S(2)}) copy-start(f32[2,256,1024]{2,1,0:T(8,128)} %get-tuple-element.56) | copy-start | bytes 6291460
  106.5 12.5 %collective-permute-start.19 = (bf16[528,256]{1,0:T(8,128)(2,1)S(1)}, bf16[528,256]{1,0:T(8,128)(2,1)S(1)}, u32[]{:S(2)}, u32[]{:S(2)}) collective-permute-start(bf16[528,256]{1,0:T(8,128)(2,1)S(1)} %fusion.7), channel_id=1, source_target_pairs={{0,4},{4,0},{8,12},{12,8},{16,20},{20,16},{24,28},{28,24},{1,5},{5... | collective-permute-start | bytes 811016 | tf_op jit(solution)/shard_map/ppermute | solution.py:29
  111.8 11.5 %collective-permute-start.24 = (bf16[528,256]{1,0:T(8,128)(2,1)S(1)}, bf16[528,256]{1,0:T(8,128)(2,1)S(1)}, u32[]{:S(2)}, u32[]{:S(2)}) collective-permute-start(bf16[528,256]{1,0:T(8,128)(2,1)S(1)} %fusion.8), channel_id=1, source_target_pairs={{0,8},{4,12},{8,0},{12,4},{16,24},{20,28},{24,16},{28,20},{1,9},{5... | collective-permute-start | bytes 811016 | tf_op jit(solution)/shard_map/ppermute | solution.py:29
  114.2 32.9 %collective-permute-start.10 = (bf16[528,256]{1,0:T(8,128)(2,1)S(1)}, bf16[528,256]{1,0:T(8,128)(2,1)S(1)}, u32[]{:S(2)}, u32[]{:S(2)}) collective-permute-start(bf16[528,256]{1,0:T(8,128)(2,1)S(1)} %fusion.3), channel_id=1, source_target_pairs={{0,16},{4,20},{8,24},{12,28},{16,0},{20,4},{24,8},{28,12},{1,17},{... | collective-permute-start | bytes 811016 | tf_op jit(solution)/shard_map/ppermute | solution.py:29
  119.0 34.0 %collective-permute-start.15 = (bf16[528,256]{1,0:T(8,128)(2,1)S(1)}, bf16[528,256]{1,0:T(8,128)(2,1)S(1)}, u32[]{:S(2)}, u32[]{:S(2)}) collective-permute-start(bf16[528,256]{1,0:T(8,128)(2,1)S(1)} %fusion.2), channel_id=1, source_target_pairs={{0,16},{4,20},{8,24},{12,28},{16,0},{20,4},{24,8},{28,12},{1,17},{... | collective-permute-start | bytes 811016 | tf_op jit(solution)/shard_map/ppermute | solution.py:29
  123.3 35.6 %collective-permute-start.20 = (bf16[528,256]{1,0:T(8,128)(2,1)S(1)}, bf16[528,256]{1,0:T(8,128)(2,1)S(1)}, u32[]{:S(2)}, u32[]{:S(2)}) collective-permute-start(bf16[528,256]{1,0:T(8,128)(2,1)S(1)} %fusion.1), channel_id=1, source_target_pairs={{0,16},{4,20},{8,24},{12,28},{16,0},{20,4},{24,8},{28,12},{1,17},{... | collective-permute-start | bytes 811016 | tf_op jit(solution)/shard_map/ppermute | solution.py:29
  125.7 36.9 %collective-permute-start.25 = (bf16[528,256]{1,0:T(8,128)(2,1)S(1)}, bf16[528,256]{1,0:T(8,128)(2,1)S(1)}, u32[]{:S(2)}, u32[]{:S(2)}) collective-permute-start(bf16[528,256]{1,0:T(8,128)(2,1)S(1)} %fusion), channel_id=1, source_target_pairs={{0,16},{4,20},{8,24},{12,28},{16,0},{20,4},{24,8},{28,12},{1,17},{... | collective-permute-start | bytes 811016 | tf_op jit(solution)/shard_map/ppermute | solution.py:29
  147.2 32.8 %collective-permute-start.7 = (bf16[1,256,1024]{2,1,0:T(8,128)(2,1)S(1)}, bf16[1,256,1024]{2,1,0:T(8,128)(2,1)S(1)}, u32[]{:S(2)}, u32[]{:S(2)}) collective-permute-start(bf16[1,256,1024]{2,1,0:T(8,128)(2,1)S(1)} %add_convert_fusion.1), channel_id=1, source_target_pairs={{0,2},{2,0},{1,3},{3,1},{4,6},{6,4},{5,7},{7,5},{8,10},{10,8},{9,1... | collective-permute-start | bytes 1572872 | tf_op jit(solution)/shard_map/ppermute | solution.py:29
  153.1 15.2 %collective-permute-start.11 = (bf16[528,256]{1,0:T(8,128)(2,1)S(1)}, bf16[528,256]{1,0:T(8,128)(2,1)S(1)}, u32[]{:S(2)}, u32[]{:S(2)}) collective-permute-start(bf16[528,256]{1,0:T(8,128)(2,1)S(1)} %add_convert_fusion.8), channel_id=1, source_target_pairs={{0,8},{4,12},{8,0},{12,4},{16,24},{20,28},{24,16},{28,20},{1,9},{5... | collective-permute-start | bytes 811016 | tf_op jit(solution)/shard_map/ppermute | solution.py:29
  158.8 9.5 %collective-permute-start.16 = (bf16[528,256]{1,0:T(8,128)(2,1)S(1)}, bf16[528,256]{1,0:T(8,128)(2,1)S(1)}, u32[]{:S(2)}, u32[]{:S(2)}) collective-permute-start(bf16[528,256]{1,0:T(8,128)(2,1)S(1)} %add_convert_fusion.6), channel_id=1, source_target_pairs={{0,4},{4,0},{8,12},{12,8},{16,20},{20,16},{24,28},{28,24},{1,5},{5... | collective-permute-start | bytes 811016 | tf_op jit(solution)/shard_map/ppermute | solution.py:29
  162.6 8.5 %collective-permute-start.21 = (bf16[528,256]{1,0:T(8,128)(2,1)S(1)}, bf16[528,256]{1,0:T(8,128)(2,1)S(1)}, u32[]{:S(2)}, u32[]{:S(2)}) collective-permute-start(bf16[528,256]{1,0:T(8,128)(2,1)S(1)} %add_convert_fusion.4), channel_id=1, source_target_pairs={{0,4},{4,0},{8,12},{12,8},{16,20},{20,16},{24,28},{28,24},{1,5},{5... | collective-permute-start | bytes 811016 | tf_op jit(solution)/shard_map/ppermute | solution.py:29
  168.3 9.4 %collective-permute-start.26 = (bf16[528,256]{1,0:T(8,128)(2,1)S(1)}, bf16[528,256]{1,0:T(8,128)(2,1)S(1)}, u32[]{:S(2)}, u32[]{:S(2)}) collective-permute-start(bf16[528,256]{1,0:T(8,128)(2,1)S(1)} %add_convert_fusion.2), channel_id=1, source_target_pairs={{0,8},{4,12},{8,0},{12,4},{16,24},{20,28},{24,16},{28,20},{1,9},{5... | collective-permute-start | bytes 811016 | tf_op jit(solution)/shard_map/ppermute | solution.py:29
  168.4 12.6 %copy-start = (bf16[2,528,256]{2,1,0:T(8,128)(2,1)}, bf16[2,528,256]{2,1,0:T(8,128)(2,1)S(1)}, u32[]{:S(2)}) copy-start(bf16[2,528,256]{2,1,0:T(8,128)(2,1)S(1)} %pad_maximum_fusion.near_ref) | copy-start | bytes 1622020
  168.4 41.9 %collective-permute-start.12 = (bf16[2,528,256]{2,1,0:T(8,128)(2,1)S(1)}, bf16[2,528,256]{2,1,0:T(8,128)(2,1)S(1)}, u32[]{:S(2)}, u32[]{:S(2)}) collective-permute-start(bf16[2,528,256]{2,1,0:T(8,128)(2,1)S(1)} %pad_maximum_fusion.near_ref), channel_id=1, source_target_pairs={{0,4},{4,0},{8,12},{12,8},{16,20},{20,16},{24,28},{28,24},{1,5},{5... | collective-permute-start | bytes 1622024 | tf_op jit(solution)/shard_map/ppermute | solution.py:29
  170.0 29.4 %copy-start.1 = (bf16[2,528,256]{2,1,0:T(8,128)(2,1)}, bf16[2,528,256]{2,1,0:T(8,128)(2,1)S(1)}, u32[]{:S(2)}) copy-start(bf16[2,528,256]{2,1,0:T(8,128)(2,1)S(1)} %pad_maximum_fusion.1.near_ref) | copy-start | bytes 1622020
  171.1 33.9 %collective-permute-start.17 = (bf16[2,528,256]{2,1,0:T(8,128)(2,1)S(1)}, bf16[2,528,256]{2,1,0:T(8,128)(2,1)S(1)}, u32[]{:S(2)}, u32[]{:S(2)}) collective-permute-start(bf16[2,528,256]{2,1,0:T(8,128)(2,1)S(1)} %pad_maximum_fusion.1.near_ref), channel_id=1, source_target_pairs={{0,8},{4,12},{8,0},{12,4},{16,24},{20,28},{24,16},{28,20},{1,9},{5... | collective-permute-start | bytes 1622024 | tf_op jit(solution)/shard_map/ppermute | solution.py:29
  172.2 27.7 %copy-start.2 = (bf16[2,528,256]{2,1,0:T(8,128)(2,1)}, bf16[2,528,256]{2,1,0:T(8,128)(2,1)S(1)}, u32[]{:S(2)}) copy-start(bf16[2,528,256]{2,1,0:T(8,128)(2,1)S(1)} %pad_maximum_fusion.2.near_ref) | copy-start | bytes 1622020
  177.7 22.2 %collective-permute-start.22 = (bf16[2,528,256]{2,1,0:T(8,128)(2,1)S(1)}, bf16[2,528,256]{2,1,0:T(8,128)(2,1)S(1)}, u32[]{:S(2)}, u32[]{:S(2)}) collective-permute-start(bf16[2,528,256]{2,1,0:T(8,128)(2,1)S(1)} %pad_maximum_fusion.2.near_ref), channel_id=1, source_target_pairs={{0,8},{4,12},{8,0},{12,4},{16,24},{20,28},{24,16},{28,20},{1,9},{5... | collective-permute-start | bytes 1622024 | tf_op jit(solution)/shard_map/ppermute | solution.py:29
  177.7 16.6 %copy-start.3 = (bf16[2,528,256]{2,1,0:T(8,128)(2,1)}, bf16[2,528,256]{2,1,0:T(8,128)(2,1)S(1)}, u32[]{:S(2)}) copy-start(bf16[2,528,256]{2,1,0:T(8,128)(2,1)S(1)} %pad_maximum_fusion.3.near_ref) | copy-start | bytes 1622020
  177.7 16.5 %collective-permute-start.27 = (bf16[2,528,256]{2,1,0:T(8,128)(2,1)S(1)}, bf16[2,528,256]{2,1,0:T(8,128)(2,1)S(1)}, u32[]{:S(2)}, u32[]{:S(2)}) collective-permute-start(bf16[2,528,256]{2,1,0:T(8,128)(2,1)S(1)} %pad_maximum_fusion.3.near_ref), channel_id=1, source_target_pairs={{0,4},{4,0},{8,12},{12,8},{16,20},{20,16},{24,28},{28,24},{1,5},{5... | collective-permute-start | bytes 1622024 | tf_op jit(solution)/shard_map/ppermute | solution.py:29
  210.3 0.8 copy-start.11
  (4 other events, 3.2 us)

commit v2 on v1

v2 whole, which is shorter than its diff:
```python
import functools
import math

import jax
import jax.numpy as jnp
from jax import lax
from jax.experimental import pallas as pl
from jax.experimental.pallas import tpu as pltpu
from jax.sharding import PartitionSpec as P


F32 = jnp.float32
BF16 = jnp.bfloat16
LANES = 128
SUBLANES = 8
LIMIT = 60000 * 2**10
BLOCKS = 4
FIRST, SECOND = (0, 1), (1, 0)
GROUPS = (((11, FIRST), (11, SECOND)), ((11, FIRST), (11, SECOND)))
CALLS = ((0,), (1,))


def chunk_rows(hidden):
    total = sum(share for group in GROUPS for share, _ in group)
    assert hidden % total == 0
    unit, start, out = hidden // total, 0, []
    for group in GROUPS:
        heights = [share * unit for share, _ in group]
        out.append((start, sum(heights), heights, [order for _, order in group]))
        start += sum(heights)
    return out


def bit_count(size):
    return size.bit_length() - 1


def exchange(value, axis, bit):
    size = lax.axis_size(axis)
    return lax.ppermute(value, axis, [(i, i ^ (1 << bit)) for i in range(size)])


FINISH = (
    (0, (0, 1)),
    (1, (0, 1)),
    (2, (0,)),
    (3, (0, 1)),
    (2, (1,)),
)


def rep_bit(bit):
    return (lax.axis_index("rep") >> bit) & 1


def dot_rows(left, right):
    return lax.dot_general(left, right, (((1,), (1,)), ((), ())), preferred_element_type=F32)


def dot(left, right):
    return lax.dot_general(left, right, (((1,), (0,)), ((), ())), preferred_element_type=F32)


def lane_index():
    return lax.broadcasted_iota(jnp.int32, (SUBLANES, LANES), 1)


def moved_later(tiles, offset):
    lane = lane_index()
    turned = [pltpu.roll(tile, offset, 1) for tile in tiles]
    before = [jnp.zeros_like(tiles[0])] + turned[:-1]
    return [jnp.where(lane < offset, b, t) for b, t in zip(before, turned)]


def moved_earlier(tiles, offset):
    lane = lane_index()
    turned = [pltpu.roll(tile, LANES - offset, 1) for tile in tiles]
    after = turned[1:] + [jnp.zeros_like(tiles[0])]
    return [jnp.where(lane >= LANES - offset, a, t) for a, t in zip(after, turned)]


def load_tiles(ref, at):
    return [ref[at, i : i + LANES] for i in range(0, ref.shape[1], LANES)]


def forward_kernel(parts, me_ref, *refs):
    pieces = refs[:parts]
    gate_ref, value_ref, gtaps_ref, vtaps_ref = refs[parts : parts + 4]
    hidden_ref, silu_ref, slope_ref, upg_ref, upv_ref = refs[parts + 4 :]
    height = gate_ref.shape[0]
    rows = pieces[0].shape[0]
    count = gtaps_ref.shape[1]
    weights = jnp.concatenate([gate_ref[...], value_ref[...]], axis=0)
    for r, piece in enumerate(pieces):
        at = pl.ds(pl.multiple_of((me_ref[0] ^ r) * rows, rows), rows)
        up = dot_rows(weights, piece[...]).astype(BF16)
        upg_ref[:, at] = up[:height]
        upv_ref[:, at] = up[height:]

    def mixed(tiles, taps_ref, at):
        total = None
        for k in range(count):
            tap = jnp.broadcast_to(taps_ref[at, k : k + 1], (SUBLANES, LANES))
            terms = [tap * tile for tile in (moved_later(tiles, k) if k else tiles)]
            total = terms if total is None else [a + b for a, b in zip(total, terms)]
        return total

    def body(i, carry):
        both = pl.ds(pl.multiple_of(i * 2 * SUBLANES, 2 * SUBLANES), 2 * SUBLANES)
        upg = [tile.astype(F32) for tile in load_tiles(upg_ref, both)]
        upv = [tile.astype(F32) for tile in load_tiles(upv_ref, both)]
        halves = []
        for half in range(2):
            rng = slice(half * SUBLANES, (half + 1) * SUBLANES)
            at = pl.ds(pl.multiple_of(i * 2 * SUBLANES + half * SUBLANES, SUBLANES), SUBLANES)
            gates = mixed([t[rng] for t in upg], gtaps_ref, at)
            values = mixed([t[rng] for t in upv], vtaps_ref, at)
            out = []
            for gate, value in zip(gates, values):
                sigma = jax.nn.sigmoid(gate)
                silu = gate * sigma
                out.append((silu * value, silu, value * sigma * (1.0 + gate * (1.0 - sigma))))
            halves.append(out)
        for n, (tops, lows) in enumerate(zip(*halves)):
            for ref, top, low in zip((hidden_ref, silu_ref, slope_ref), tops, lows):
                ref[both, n * LANES : (n + 1) * LANES] = jnp.concatenate([top, low], axis=0).astype(ref.dtype)
        return carry

    lax.fori_loop(0, height // (2 * SUBLANES), body, 0)


def forward_part(me, pieces, gate_t, value_t, gtaps, vtaps):
    hidden, model = gate_t.shape
    parts, rows = len(pieces), pieces[0].shape[0]
    tokens, count = parts * rows, gtaps.shape[1]
    height = hidden // BLOCKS
    piece = pl.BlockSpec((rows, model), lambda i, me_ref: (0, 0))
    weight = pl.BlockSpec((height, model), lambda i, me_ref: (i, 0))
    taps = pl.BlockSpec((height, count), lambda i, me_ref: (i, 0))
    out = pl.BlockSpec((height, tokens), lambda i, me_ref: (i, 0))
    return pl.pallas_call(
        functools.partial(forward_kernel, parts),
        out_shape=tuple(jax.ShapeDtypeStruct((hidden, tokens), t) for t in (BF16, F32, F32, BF16, BF16)),
        grid_spec=pltpu.PrefetchScalarGridSpec(
            num_scalar_prefetch=1,
            grid=(BLOCKS,),
            in_specs=[piece] * parts + [weight, weight, taps, taps],
            out_specs=(out,) * 5,
        ),
        compiler_params=pltpu.CompilerParams(dimension_semantics=("arbitrary",), vmem_limit_bytes=LIMIT),
        cost_estimate=pl.CostEstimate(
            flops=4 * hidden * tokens * model, bytes_accessed=18 * hidden * tokens, transcendentals=2 * hidden * tokens
        ),
        name="forward_part",
    )(me, *pieces, gate_t, value_t, gtaps, vtaps)


def backward_kernel(parts, groups, me_ref, *refs):
    refs = list(refs)

    def take(count):
        taken, refs[:count] = refs[:count], []
        return taken

    outs_count = sum(2 * len(group[2]) for group in groups)
    sources = take(2 * parts + 6)
    gtaps_ref, vtaps_ref = take(2)
    targets = take(outs_count + 2)
    all_sums = take(len(groups))
    toks, cots, bufs = take(parts), take(parts), take(6)
    outs, grads, (back, acc, in_sems, out_sems) = take(outs_count), take(2), take(4)
    rows = toks[0].shape[0]
    count = gtaps_ref.shape[1]
    offset = groups[0][0]

    started, arrivals, leaving = {}, {}, []
    for n, (src, dst) in enumerate(zip(sources[: 2 * parts], toks + cots)):
        arrivals[n] = (src, dst)
    for g, (start, height, _, _) in enumerate(groups):
        for n, (src, dst) in enumerate(zip(sources[2 * parts :], bufs)):
            arrivals[g, n] = (src.at[pl.ds(start, height)], dst.at[pl.ds(start - offset, height)])

    def begin(*keys):
        for key in keys:
            src, dst = arrivals[key]
            started[key] = pltpu.make_async_copy(src, dst, in_sems.at[len(started)])
            started[key].start()

    def arrived(*keys):
        for key in keys:
            started[key].wait()

    def leave(src, dst):
        copy = pltpu.make_async_copy(src, dst, out_sems.at[len(leaving)])
        copy.start()
        leaving.append(copy)

    spots = [pl.ds(pl.multiple_of((me_ref[0] ^ r) * rows, rows), rows) for r in range(parts)]
    fields = (2, 3, 4, 5)
    begin((0, 0), *range(parts, 2 * parts), *[(0, n) for n in fields])
    base_out = 0
    for g, (start, height, heights, orders) in enumerate(groups):
        low = start - offset
        down_ref, hidden_ref, silu_ref, slope_ref, upg_ref, upv_ref = [buf.at[low : low + height] for buf in bufs]
        ggrad_ref, vgrad_ref = [grad.at[low : low + height] for grad in grads]
        gtaps, vtaps = gtaps_ref.at[low : low + height], vtaps_ref.at[low : low + height]
        arrived((g, 0))
        for r, (at, piece) in enumerate(zip(spots, cots)):
            if g == 0:
                arrived(parts + r)
            back[:height, at] = dot_rows(down_ref[...], piece[...])
        begin((g, 1), *(range(parts) if g == 0 else ()))
        if g + 1 < len(groups):
            begin((g + 1, 0), *[(g + 1, n) for n in fields])
        arrived(*[(g, n) for n in fields])

        def mixed(tiles, fields, taps_ref, at, first):
            total = None
            for k in range(count):
                tap = jnp.broadcast_to(taps_ref[at, k : k + 1], (SUBLANES, LANES))
                moved = moved_earlier(tiles, k) if k else tiles
                terms = [tap * tile for tile in moved]
                total = terms if total is None else [a + b for a, b in zip(total, terms)]
                acc[first + k, at] = sum(m * f for m, f in zip(moved, fields))
            return total

        def body(i, carry):
            both = pl.ds(pl.multiple_of(i * 2 * SUBLANES, 2 * SUBLANES), 2 * SUBLANES)
            upg = [tile.astype(F32) for tile in load_tiles(upg_ref, both)]
            upv = [tile.astype(F32) for tile in load_tiles(upv_ref, both)]
            gates, values = [], []
            for half in range(2):
                rng = slice(half * SUBLANES, (half + 1) * SUBLANES)
                at = pl.ds(pl.multiple_of(i * 2 * SUBLANES + half * SUBLANES, SUBLANES), SUBLANES)
                up = load_tiles(back, at)
                gback = [a * b for a, b in zip(up, load_tiles(slope_ref, at))]
                gates.append(mixed(gback, [t[rng] for t in upg], gtaps, at, 0))
                vback = [a * b for a, b in zip(up, load_tiles(silu_ref, at))]
                values.append(mixed(vback, [t[rng] for t in upv], vtaps, at, count))
            for ref, halves in ((ggrad_ref, gates), (vgrad_ref, values)):
                for n, (top, bottom) in enumerate(zip(*halves)):
                    ref[both, n * LANES : (n + 1) * LANES] = jnp.concatenate([top, bottom], axis=0).astype(BF16)
            return carry

        lax.fori_loop(0, height // (2 * SUBLANES), body, 0)
        leave(ggrad_ref, targets[outs_count].at[low : low + height])
        leave(vgrad_ref, targets[outs_count + 1].at[low : low + height])
        arrived((g, 1), *(range(parts) if g == 0 else ()))

        size = outs[0].shape[2]
        for pair in (3, 2, 1, 0):
            bits = (pair >> 1, pair & 1)
            cols = pl.ds(pl.multiple_of((me_ref[1] ^ pair) * size, size), size)
            both, down = None, None
            for at, tok, cot in zip(spots, toks, cots):
                term = dot(jnp.concatenate([ggrad_ref[:, at], vgrad_ref[:, at]], axis=0), tok[:, cols])
                both = term if both is None else both + term
                term = dot(hidden_ref[:, at], cot[:, cols])
                down = term if down is None else down + term
            both, down = both.astype(BF16), down.astype(BF16)
            top = 0
            for sub, (part, (first, second)) in enumerate(zip(heights, orders)):
                which, spot = base_out + 2 * sub + 1 - bits[first], bits[second]
                ref, own = outs[which], slice(top, top + part)
                ref[spot, :part] = both[own]
                ref[spot, part : 2 * part] = both[height:][own]
                ref[spot, 2 * part :] = down[own]
                leave(ref.at[spot], targets[which].at[spot])
                top += part
        ones = jnp.ones((SUBLANES, LANES), F32)
        for k in range(2 * count):
            total = lax.dot_general(
                ones, acc[k, :height], (((1,), (1,)), ((), ())), precision=lax.Precision.HIGHEST, preferred_element_type=F32
            )
            all_sums[g][k : k + 1] = total[:1]
        base_out += 2 * len(heights)
    for copy in leaving:
        copy.wait()


def backward_part(groups, me, toks, cots, down, hidden, silu, slope, upg, upv, gtaps, vtaps):
    model = down.shape[1]
    parts, rows = len(toks), toks[0].shape[0]
    tokens, count = parts * rows, gtaps.shape[1]
    height, most = sum(group[1] for group in groups), max(group[1] for group in groups)
    offset = groups[0][0]
    payloads = [(2, 3 * part, model // 4) for group in groups for part in group[2] for _ in range(2)]
    anywhere = pl.BlockSpec(memory_space=pl.ANY)
    vmem = pl.BlockSpec(memory_space=pltpu.VMEM)
    sums = [(2 * count, group[1]) for group in groups]
    shapes = (*payloads, (height, tokens), (height, tokens), *sums)
    types = (BF16,) * (len(payloads) + 2) + (F32,) * len(sums)
    mine = slice(offset, offset + height)
    return pl.pallas_call(
        functools.partial(backward_kernel, parts, groups),
        out_shape=tuple(jax.ShapeDtypeStruct(s, t) for s, t in zip(shapes, types)),
        grid_spec=pltpu.PrefetchScalarGridSpec(
            num_scalar_prefetch=1,
            grid=(1,),
            in_specs=[anywhere] * (2 * parts + 6) + [vmem, vmem],
            out_specs=(anywhere,) * (len(payloads) + 2) + (vmem,) * len(sums),
            scratch_shapes=[
                *[pltpu.VMEM((rows, model), BF16)] * (2 * parts),
                pltpu.VMEM((height, model), BF16),
                *[pltpu.VMEM((height, tokens), t) for t in (BF16, F32, F32, BF16, BF16)],
                *[pltpu.VMEM(shape, BF16) for shape in payloads],
                *[pltpu.VMEM((height, tokens), BF16)] * 2,
                pltpu.VMEM((most, tokens), F32),
                pltpu.VMEM((2 * count, most, LANES), F32),
                pltpu.SemaphoreType.DMA((2 * parts + 6 * len(groups),)),
                pltpu.SemaphoreType.DMA((2 * len(payloads) + 2 * len(groups),)),
            ],
        ),
        compiler_params=pltpu.CompilerParams(dimension_semantics=("arbitrary",), vmem_limit_bytes=LIMIT),
        cost_estimate=pl.CostEstimate(
            flops=8 * height * tokens * model, bytes_accessed=8 * tokens * model, transcendentals=0
        ),
        name="backward_part",
    )(me, *toks, *cots, down, hidden, silu, slope, upg, upv, gtaps[mine], vtaps[mine])


def input_kernel(me_ref, *refs):
    count = (len(refs) - 3) // 2
    ggrads, vgrads = refs[:count], refs[count : 2 * count]
    gate_ref, value_ref, out_ref = refs[2 * count :]
    total = None
    for grads, weight_ref in ((ggrads, gate_ref), (vgrads, value_ref)):
        low = 0
        for ref in grads:
            high = low + ref.shape[0]
            term = lax.dot_general(
                ref[...], weight_ref[low:high], (((0,), (0,)), ((), ())), preferred_element_type=F32
            )
            total = term if total is None else total + term
            low = high
    out_ref[0] = total.astype(out_ref.dtype)


def input_part(me, ggrads, vgrads, gate_t, value_t, parts, odd, dtype):
    hidden, model = gate_t.shape
    tokens = ggrads[0].shape[1]
    rows, half = tokens // parts, parts // 2
    fields = [pl.BlockSpec((g.shape[0], rows), lambda i, me_ref: (0, me_ref[0] ^ (2 * i + odd))) for g in ggrads]
    weight = pl.BlockSpec((hidden, model), lambda i, me_ref: (0, 0))
    return pl.pallas_call(
        input_kernel,
        out_shape=jax.ShapeDtypeStruct((half, rows, model), dtype),
        grid_spec=pltpu.PrefetchScalarGridSpec(
            num_scalar_prefetch=1,
            grid=(half,),
            in_specs=fields * 2 + [weight, weight],
            out_specs=pl.BlockSpec((1, rows, model), lambda i, me_ref: (i, 0, 0)),
        ),
        compiler_params=pltpu.CompilerParams(dimension_semantics=("arbitrary",), vmem_limit_bytes=LIMIT),
        cost_estimate=pl.CostEstimate(
            flops=2 * hidden * tokens * model, bytes_accessed=2 * hidden * tokens + 3 * tokens * model, transcendentals=0
        ),
        name="input_part",
    )(me, *ggrads, *vgrads, gate_t, value_t)


def add(left, right, dtype):
    return (left.astype(F32) + right.astype(F32)).astype(dtype)


def reduce_chunk(sent, kept, first, second):
    got = exchange(sent, "rep", first)
    half = add(kept[1], got[1], BF16)
    over = exchange(half, "rep", second)
    mine = add(add(kept[0], got[0], F32), over, BF16)
    rest = [b for b in range(bit_count(lax.axis_size("rep"))) if b not in (first, second)]
    for at, bit in enumerate(rest):
        theirs = exchange(mine, "rep", bit)
        mine = add(mine, theirs, BF16 if at == len(rest) - 1 else F32)
    other = exchange(mine, "rep", second)
    pair = jnp.stack([mine, other])
    return pair, exchange(pair, "rep", first)


def place_kernel(scale, start, sides, swap, count, where_ref, *refs):
    pairs, refs = refs[: len(sides)], refs[len(sides) :]
    outs, (stage, out_sems) = refs[count : count + 3], refs[count + 3 :]
    height, size = stage.shape[2:]
    leaving = []
    for i, (pair, spot) in enumerate((pair.at[i], 2 * side + i) for pair, side in zip(pairs, sides) for i in range(2)):
        spot = ((spot >> 1) | ((spot & 1) << 1) if swap else spot) ^ where_ref[1]
        cols = pl.ds(pl.multiple_of(spot * size, size), size)
        for n, out_ref in enumerate(outs):
            stage[i, n] = pair[n * height : (n + 1) * height].astype(F32) * scale
            copy = pltpu.make_async_copy(stage.at[i, n], out_ref.at[pl.ds(start, height), cols], out_sems.at[i, n])
            copy.start()
            leaving.append(copy)
    for copy in leaving:
        copy.wait()


def place(start, height, sides, swap, where, pairs, outs, shape, scale):
    model = shape[1]
    anywhere = pl.BlockSpec(memory_space=pl.ANY)
    blocks = 2 * len(sides)
    return pl.pallas_call(
        functools.partial(place_kernel, scale, start, sides, swap, len(outs)),
        out_shape=(jax.ShapeDtypeStruct(shape, F32),) * 3,
        grid_spec=pltpu.PrefetchScalarGridSpec(
            num_scalar_prefetch=1,
            grid=(1,),
            in_specs=[pl.BlockSpec(memory_space=pltpu.VMEM)] * len(pairs) + [anywhere] * len(outs),
            out_specs=(anywhere,) * 3,
            scratch_shapes=[
                pltpu.VMEM((blocks, 3, height, model // 4), F32),
                pltpu.SemaphoreType.DMA((blocks, 3)),
            ],
        ),
        input_output_aliases={1 + len(pairs) + n: n for n in range(len(outs))},
        compiler_params=pltpu.CompilerParams(dimension_semantics=("arbitrary",), vmem_limit_bytes=LIMIT // 4),
        cost_estimate=pl.CostEstimate(
            flops=3 * height * model, bytes_accessed=9 * blocks // 2 * height * model, transcendentals=0
        ),
        name="place",
    )(where, *pairs, *outs)


def butterfly(value):
    for bit in range(bit_count(lax.axis_size("rep"))):
        value = value + exchange(value, "rep", bit)
    return value


def gather_relative(own):
    found = {0: own}
    base = bit_count(lax.axis_size("tp"))
    for bit in range(bit_count(lax.axis_size("fs"))):
        found.update({r | (1 << (base + bit)): exchange(item, "fs", bit) for r, item in list(found.items())})
    for bit in range(base):
        found.update({r | (1 << bit): exchange(item, "tp", bit) for r, item in list(found.items())})
    return [found[r] for r in range(len(found))]


def scatter_relative(sent, kept):
    moved = exchange(sent, "tp", 0)
    blocks = [add(kept[i], moved[i], F32) for i in range(kept.shape[0])]
    bits = [("tp", b) for b in range(1, bit_count(lax.axis_size("tp")))]
    bits += [("fs", b) for b in range(bit_count(lax.axis_size("fs")))]
    for axis, bit in bits:
        far = jnp.stack(blocks[1::2]).astype(BF16)
        moved = exchange(far, axis, bit)
        blocks = [add(item, moved[i], F32) for i, item in enumerate(blocks[0::2])]
    return blocks[0].astype(BF16)


def layer(tokens, cotangent, gate_weight, value_weight, down_weight, gate_taps, value_taps):
    rows, model = tokens.shape
    hidden = gate_weight.shape[1]
    parts = lax.axis_size("fs") * lax.axis_size("tp")
    scale = 1.0 / math.sqrt(rows * parts * lax.axis_size("rep"))
    me = (lax.axis_index("fs") * lax.axis_size("tp") + lax.axis_index("tp")).astype(jnp.int32)
    gate_t, value_t = gate_weight.T, value_weight.T
    gtaps, vtaps = gate_taps.T, value_taps.T
    where = jnp.stack([me, (2 * rep_bit(0) + rep_bit(1)).astype(jnp.int32)])

    cotangent, where, gtaps, vtaps = lax.optimization_barrier((cotangent, where, gtaps, vtaps))
    toks = gather_relative(tokens)
    cots = gather_relative(cotangent)
    fields = forward_part(where, toks, gate_t, value_t, gtaps, vtaps)
    ggrads, vgrads, sums, chunks = [], [], [], []
    groups = chunk_rows(hidden)
    for members in CALLS:
        mine = [groups[g] for g in members]
        found = backward_part(mine, where, toks, cots, down_weight, *fields, gtaps, vtaps)
        *payload, ggrad, vgrad = found[: len(found) - len(mine)]
        sums.extend(found[len(found) - len(mine) :])
        for start, _, heights, orders in mine:
            for height, order in zip(heights, orders):
                sent, kept, *payload = payload
                pairs = reduce_chunk(sent, kept, *order)
                chunks.append((start, height, order[0] == 1, pairs))
                start += height
        ggrads.append(ggrad)
        vgrads.append(vgrad)
    outs = ()
    for chunk, sides in FINISH:
        start, height, swap, pairs = chunks[chunk]
        picked = [pairs[side] for side in sides]
        outs = place(start, height, sides, swap, where, picked, outs, (hidden, model), scale)
    sums = butterfly(jnp.concatenate(sums, axis=1)) * scale
    away = input_part(where, ggrads, vgrads, gate_t, value_t, parts, 1, BF16)
    own = input_part(where, ggrads, vgrads, gate_t, value_t, parts, 0, F32)
    input_grad = scatter_relative(away, own)
    count = gate_taps.shape[0]
    return input_grad, outs[0].T, outs[1].T, outs[2], sums[:count], sums[count:]


def solution(mesh):
    in_specs = (
        P(("rep", "fs", "tp"), None),
        P(("rep", "fs", "tp"), None),
        P(None, ("fs", "tp")),
        P(None, ("fs", "tp")),
        P(("fs", "tp"), None),
        P(None, ("fs", "tp")),
        P(None, ("fs", "tp")),
    )
    out_specs = (
        P(("rep", "fs", "tp"), None),
        P(None, ("fs", "tp")),
        P(None, ("fs", "tp")),
        P(("fs", "tp"), None),
        P(None, ("fs", "tp")),
        P(None, ("fs", "tp")),
    )
    return jax.shard_map(layer, mesh=mesh, in_specs=in_specs, out_specs=out_specs, check_vma=False)
```

time: 216 us -> 208 us (0.963)
  local copies, waits for them, and re-layouts: 11.1 us -> 5.35 us
  Pallas kernels: 67.9 us -> 63 us
    pallas_call x7 -> x9, Pallas kernels: 53.4 us -> 48.3 us  [the longest x2 26.3 us: backward_part(): pl.pallas_call(functools.partial(backward_kernel, parts, groups), out_sha...]
    unnamed x44 -> x38, local copies, waits for them, and re-layouts: 8.51 us -> 3.82 us
  transfers between devices with their start and end apart: 31 -> 31, of which waited for: 17 -> 16; matrix products, arithmetic and copies ran while one was open for 3% -> 4% of each run, Pallas kernels for 17% -> 23%
where the time goes in v2:
time: 208 us; the launch traced here: 207 us
  waiting for transfers between devices  102 us (49%)
  Pallas kernels  63 us (30%)
  starting transfers between devices  31.5 us (15%)
  local copies, waits for them, and re-layouts  5.35 us (3%)
  other arithmetic  4 us (2%)
    ppermute x31, waiting for transfers between devices, exchange(): return lax.ppermute(value, axis, [(i, i ^ 1 << bit) for i in range(size)])  102 us
    ppermute x31, starting transfers between devices, exchange(): return lax.ppermute(value, axis, [(i, i ^ 1 << bit) for i in range(size)])  31.5 us
    pallas_call x2, Pallas kernels, backward_part(): pl.pallas_call(functools.partial(backward_kernel, parts, groups), out_sha...  26.3 us
    pallas_call x1, Pallas kernels, forward_part(): pl.pallas_call(functools.partial(forward_kernel, parts), out_shape=tuple(...  14.7 us
    pallas_call x2, Pallas kernels, input_part(): pl.pallas_call(input_kernel, out_shape=jax.ShapeDtypeStruct((half, rows,...  12.9 us
    pallas_call x5, Pallas kernels, place(): pl.pallas_call(functools.partial(place_kernel, scale, start, sides, swap,...  9.11 us
  transfers between devices with their start and end apart: 31, of which 16 were waited for; matrix products, arithmetic and copies ran while one was open for 4% of the time, Pallas kernels for 23%

profile of v2, /device:TPU:0, one launch (start us, length us, event | category | flops | bytes accessed | tf_op | source)
XLA Modules:
  0.0 207.4 jit_solution(1121268704344165831)
XLA Ops:
  0.6 3.0 %collective-permute-start.1 = (bf16[256,1024]{1,0:T(8,128)(2,1)}, bf16[256,1024]{1,0:T(8,128)(2,1)S(1)}, u32[]{:S(2)}, u32[]{:S(2)}) collective-permute-start(bf16[256,1024]{1,0:T(8,128)(2,1)} %refs_0_.5), channel_id=1, source_target_pairs={{0,2},{2,0},{1,3},{3,1},{4,6},{6,4},{5,7},{7,5},{8,10},{10,8},{9,1... | collective-permute-start | bytes 1572872 | tf_op jit(solution)/shard_map/ppermute | solution.py:40
  3.7 0.9 copy.25
  4.6 0.9 copy.26
  6.2 10.4 %collective-permute-done.1.refs_2_ = bf16[256,1024]{1,0:T(8,128)(2,1)S(1)} collective-permute-done((bf16[256,1024]{1,0:T(8,128)(2,1)}, bf16[256,1024]{1,0:T(8,128)(2,1)S(1)}, u32[]{:S(2)}, u32[]{:S(2)}) %collective-permute-start.1) | collective-permute-done | bytes 524320 | tf_op jit(solution)/shard_map/ppermute | solution.py:40
  17.2 9.9 %collective-permute-done.4.refs_6_ = bf16[256,1024]{1,0:T(8,128)(2,1)S(1)} collective-permute-done((bf16[256,1024]{1,0:T(8,128)(2,1)}, bf16[256,1024]{1,0:T(8,128)(2,1)S(1)}, u32[]{:S(2)}, u32[]{:S(2)}) %collective-permute-start.4) | collective-permute-done | bytes 524320 | tf_op jit(solution)/shard_map/ppermute | solution.py:40
  27.0 0.9 fusion.13
  29.0 14.7 %forward_part.1 = (bf16[704,1024]{1,0:T(8,128)(2,1)}, f32[704,1024]{1,0:T(8,128)}, f32[704,1024]{1,0:T(8,128)}, bf16[704,1024]{1,0:T(8,128)(2,1)}, bf16[704,1024]{1,0:T(8,128)(2,1)}) custom-call(s32[2]{0:T(128)} %pad_add_fusion.me_ref.where_ref, bf16[256,1024]{1,0:T(8,128)(2,1)} %refs_0_.5, bf16[256,1024]{1,0:T(8,128)(2,1)} %copy-done.4, ...), custom_call_target="tpu_custom_call" | custom-call | flops 2952790016 | bytes 12976128 | tf_op jit(solution)/shard_map/forward_part/pallas_call | solution.py:141
  43.7 0.8 copy-done.6
  44.7 13.1 %backward_part.3 = (bf16[2,528,256]{2,1,0:T(8,128)(2,1)}, bf16[2,528,256]{2,1,0:T(8,128)(2,1)}, bf16[2,528,256]{2,1,0:T(8,128)(2,1)}, bf16[2,528,256]{2,1,0:T(8,...) custom-call(s32[2]{0:T(128)} %pad_add_fusion.me_ref.where_ref, ...), custom_call_target="tpu_custom_call" | custom-call | flops 2952790016 | bytes 8388608 | tf_op jit(solution)/shard_map/backward_part/pallas_call | solution.py:294
  57.8 1.8 collective-permute-start.8
  59.7 13.2 %backward_part.2 = (bf16[2,528,256]{2,1,0:T(8,128)(2,1)}, bf16[2,528,256]{2,1,0:T(8,128)(2,1)}, bf16[2,528,256]{2,1,0:T(8,128)(2,1)}, bf16[2,528,256]{2,1,0:T(8,...) custom-call(s32[2]{0:T(128)} %pad_add_fusion.me_ref.where_ref, ...), custom_call_target="tpu_custom_call" | custom-call | flops 2952790016 | bytes 8388608 | tf_op jit(solution)/shard_map/backward_part/pallas_call | solution.py:294
  72.9 0.8 pad_maximum_fusion.4
  74.0 1.8 collective-permute-start.13
  76.0 6.4 %input_part.3 = bf16[2,256,1024]{2,1,0:T(8,128)(2,1)} custom-call(s32[2]{0:T(128)} %pad_add_fusion.me_ref.where_ref, bf16[352,1024]{1,0:T(8,128)(2,1)} %get-tuple-element.53.refs_0_, bf16[352,1024]{1,0:T(8,128)(2,1)} %get-tuple-element.54.refs_1_, bf16[352,1024]{1,0:T(8,128)(2,1)} %get-tuple-element.55.refs_2_, bf16[352,1024]{1,0:T(8,128)(2,1)} %get-tuple-element.56.refs_3_, ...), custom_call_target="tpu_custom_call" | custom-call | flops 1476395008 | bytes 4587520 | tf_op jit(solution)/shard_map/input_part/pallas_call | solution.py:345
  82.5 1.9 collective-permute-start.29
  84.4 6.5 %input_part.2 = f32[2,256,1024]{2,1,0:T(8,128)} custom-call(s32[2]{0:T(128)} %pad_add_fusion.me_ref.where_ref, bf16[352,1024]{1,0:T(8,128)(2,1)} %get-tuple-element.53.refs_0_, bf16[352,1024]{1,0:T(8,128)(2,1)} %get-tuple-element.54.refs_1_, bf16[352,1024]{1,0:T(8,128)(2,1)} %get-tuple-element.55.refs_2_, bf16[352,1024]{1,0:T(8,128)(2,1)} %get-tuple-element.56.refs_3_, ...), custom_call_target="tpu_custom_call" | custom-call | flops 1476395008 | bytes 4587520 | tf_op jit(solution)/shard_map/input_part/pallas_call | solution.py:345
  90.9 1.6 collective-permute-start.23
  92.4 8.0 %collective-permute-done.29 = f32[6,704]{1,0:T(8,128)S(1)} collective-permute-done((f32[6,704]{1,0:T(8,128)S(1)}, f32[6,704]{1,0:T(8,128)S(1)}, u32[]{:S(2)}, u32[]{:S(2)}) %collective-permute-start.29) | collective-permute-done | bytes 16928 | tf_op jit(solution)/shard_map/ppermute | solution.py:40
  100.4 2.8 %collective-permute-start.30 = (f32[6,704]{1,0:T(8,128)S(1)}, f32[6,704]{1,0:T(8,128)S(1)}, u32[]{:S(2)}, u32[]{:S(2)}) collective-permute-start(f32[6,704]{1,0:T(8,128)S(1)} %add.117), channel_id=1, source_target_pairs={{0,16},{4,20},{8,24},{12,28},{16,0},{20,4},{24,8},{28,12},{1,17},{... | collective-permute-start | bytes 50696 | tf_op jit(solution)/shard_map/ppermute | solution.py:40
  103.3 1.6 collective-permute-start.9
  105.0 1.6 collective-permute-start.14
  107.4 4.6 %collective-permute-done.9 = bf16[528,256]{1,0:T(8,128)(2,1)S(1)} collective-permute-done((bf16[528,256]{1,0:T(8,128)(2,1)S(1)}, bf16[528,256]{1,0:T(8,128)(2,1)S(1)}, u32[]{:S(2)}, u32[]{:S(2)}) %collective-permute-start.9) | collective-permute-done | bytes 270368 | tf_op jit(solution)/shard_map/ppermute | solution.py:40
  112.0 1.6 collective-permute-start.24
  113.7 0.8 collective-permute-done.14
  114.9 4.3 %collective-permute-done.19 = bf16[528,256]{1,0:T(8,128)(2,1)S(1)} collective-permute-done((bf16[528,256]{1,0:T(8,128)(2,1)S(1)}, bf16[528,256]{1,0:T(8,128)(2,1)S(1)}, u32[]{:S(2)}, u32[]{:S(2)}) %collective-permute-start.19) | collective-permute-done | bytes 270368 | tf_op jit(solution)/shard_map/ppermute | solution.py:40
  119.7 3.8 %collective-permute-done.24 = bf16[528,256]{1,0:T(8,128)(2,1)S(1)} collective-permute-done((bf16[528,256]{1,0:T(8,128)(2,1)S(1)}, bf16[528,256]{1,0:T(8,128)(2,1)S(1)}, u32[]{:S(2)}, u32[]{:S(2)}) %collective-permute-start.24) | collective-permute-done | bytes 270368 | tf_op jit(solution)/shard_map/ppermute | solution.py:40
  123.5 2.3 %collective-permute-start.20 = (bf16[528,256]{1,0:T(8,128)(2,1)S(1)}, bf16[528,256]{1,0:T(8,128)(2,1)S(1)}, u32[]{:S(2)}, u32[]{:S(2)}) collective-permute-start(bf16[528,256]{1,0:T(8,128)(2,1)S(1)} %fusion.4), channel_id=1, source_target_pairs={{0,16},{4,20},{8,24},{12,28},{16,0},{20,4},{24,8},{28,12},{1,17},{... | collective-permute-start | bytes 811016 | tf_op jit(solution)/shard_map/ppermute | solution.py:40
  126.8 20.6 %collective-permute-done.10 = bf16[528,256]{1,0:T(8,128)(2,1)S(1)} collective-permute-done((bf16[528,256]{1,0:T(8,128)(2,1)S(1)}, bf16[528,256]{1,0:T(8,128)(2,1)S(1)}, u32[]{:S(2)}, u32[]{:S(2)}) %collective-permute-start.10) | collective-permute-done | bytes 270368 | tf_op jit(solution)/shard_map/ppermute | solution.py:40
  147.4 1.5 collective-permute-start.7
  148.9 4.4 %collective-permute-done.15 = bf16[528,256]{1,0:T(8,128)(2,1)S(1)} collective-permute-done((bf16[528,256]{1,0:T(8,128)(2,1)S(1)}, bf16[528,256]{1,0:T(8,128)(2,1)S(1)}, u32[]{:S(2)}, u32[]{:S(2)}) %collective-permute-start.15) | collective-permute-done | bytes 270368 | tf_op jit(solution)/shard_map/ppermute | solution.py:40
  153.4 5.7 %collective-permute-done.20 = bf16[528,256]{1,0:T(8,128)(2,1)S(1)} collective-permute-done((bf16[528,256]{1,0:T(8,128)(2,1)S(1)}, bf16[528,256]{1,0:T(8,128)(2,1)S(1)}, u32[]{:S(2)}, u32[]{:S(2)}) %collective-permute-start.20) | collective-permute-done | bytes 270368 | tf_op jit(solution)/shard_map/ppermute | solution.py:40
  159.1 1.5 collective-permute-start.16
  160.6 2.2 %collective-permute-done.25 = bf16[528,256]{1,0:T(8,128)(2,1)S(1)} collective-permute-done((bf16[528,256]{1,0:T(8,128)(2,1)S(1)}, bf16[528,256]{1,0:T(8,128)(2,1)S(1)}, u32[]{:S(2)}, u32[]{:S(2)}) %collective-permute-start.25) | collective-permute-done | bytes 270368 | tf_op jit(solution)/shard_map/ppermute | solution.py:40
  162.8 1.5 collective-permute-start.21
  164.4 4.1 %collective-permute-done.11 = bf16[528,256]{1,0:T(8,128)(2,1)S(1)} collective-permute-done((bf16[528,256]{1,0:T(8,128)(2,1)S(1)}, bf16[528,256]{1,0:T(8,128)(2,1)S(1)}, u32[]{:S(2)}, u32[]{:S(2)}) %collective-permute-start.11) | collective-permute-done | bytes 270368 | tf_op jit(solution)/shard_map/ppermute | solution.py:40
  168.6 1.6 collective-permute-start.12
  170.2 1.2 collective-permute-done.21
  171.4 0.9 collective-permute-start.17
  172.4 5.5 %collective-permute-done.26 = bf16[528,256]{1,0:T(8,128)(2,1)S(1)} collective-permute-done((bf16[528,256]{1,0:T(8,128)(2,1)S(1)}, bf16[528,256]{1,0:T(8,128)(2,1)S(1)}, u32[]{:S(2)}, u32[]{:S(2)}) %collective-permute-start.26) | collective-permute-done | bytes 270368 | tf_op jit(solution)/shard_map/ppermute | solution.py:40
  178.0 1.6 collective-permute-start.27
  180.1 1.0 fusion.7
  181.2 13.3 %collective-permute-done.27.refs_1_ = bf16[2,528,256]{2,1,0:T(8,128)(2,1)S(1)} collective-permute-done((bf16[2,528,256]{2,1,0:T(8,128)(2,1)S(1)}, bf16[2,528,256]{2,1,0:T(8,128)(2,1)S(1)}, u32[]{:S(2)}, u32[]{:S(2)}) %collective-permute-start.27) | collective-permute-done | bytes 540704 | tf_op jit(solution)/shard_map/ppermute | solution.py:40
  194.5 2.0 place.5
  196.5 3.6 %collective-permute-done.22.refs_1_ = bf16[2,528,256]{2,1,0:T(8,128)(2,1)S(1)} collective-permute-done((bf16[2,528,256]{2,1,0:T(8,128)(2,1)S(1)}, bf16[2,528,256]{2,1,0:T(8,128)(2,1)S(1)}, u32[]{:S(2)}, u32[]{:S(2)}) %collective-permute-start.22) | collective-permute-done | bytes 540704 | tf_op jit(solution)/shard_map/ppermute | solution.py:40
  200.1 2.0 place.6
  202.1 1.6 place.7
  203.7 2.0 place.8
  205.7 1.6 place.9
  (87 shorter events, 7.0 us)
Async XLA Ops:
  0.6 16.0 %collective-permute-start.1 = (bf16[256,1024]{1,0:T(8,128)(2,1)}, bf16[256,1024]{1,0:T(8,128)(2,1)S(1)}, u32[]{:S(2)}, u32[]{:S(2)}) collective-permute-start(bf16[256,1024]{1,0:T(8,128)(2,1)} %refs_0_.5), channel_id=1, source_target_pairs={{0,2},{2,0},{1,3},{3,1},{4,6},{6,4},{5,7},{7,5},{8,10},{10,8},{9,1... | collective-permute-start | bytes 1572872 | tf_op jit(solution)/shard_map/ppermute | solution.py:40
  4.5 23.4 %copy-start.8 = (f32[3,704]{0,1:T(8,128)}, f32[3,704]{0,1:T(8,128)S(1)}, u32[]{:S(2)}) copy-start(f32[3,704]{0,1:T(8,128)S(1)} %copy.25) | copy-start | bytes 25348
  5.5 22.5 %copy-start.9 = (f32[3,704]{0,1:T(8,128)}, f32[3,704]{0,1:T(8,128)S(1)}, u32[]{:S(2)}) copy-start(f32[3,704]{0,1:T(8,128)S(1)} %copy.26) | copy-start | bytes 25348
  6.2 20.8 %collective-permute-start.4 = (bf16[256,1024]{1,0:T(8,128)(2,1)}, bf16[256,1024]{1,0:T(8,128)(2,1)S(1)}, u32[]{:S(2)}, u32[]{:S(2)}) collective-permute-start(bf16[256,1024]{1,0:T(8,128)(2,1)} %refs_4_.1), channel_id=1, source_target_pairs={{0,2},{2,0},{1,3},{3,1},{4,6},{6,4},{5,7},{7,5},{8,10},{10,8},{9,1... | collective-permute-start | bytes 1572872 | tf_op jit(solution)/shard_map/ppermute | solution.py:40
  6.2 21.7 %collective-permute-start = (bf16[256,1024]{1,0:T(8,128)(2,1)}, bf16[256,1024]{1,0:T(8,128)(2,1)S(1)}, u32[]{:S(2)}, u32[]{:S(2)}) collective-permute-start(bf16[256,1024]{1,0:T(8,128)(2,1)} %refs_0_.5), channel_id=1, source_target_pairs={{0,1},{1,0},{2,3},{3,2},{4,5},{5,4},{6,7},{7,6},{8,9},{9,8},{10,11... | collective-permute-start | bytes 1572872 | tf_op jit(solution)/shard_map/ppermute | solution.py:40
  16.6 11.3 %copy-start.2 = (bf16[256,1024]{1,0:T(8,128)(2,1)}, bf16[256,1024]{1,0:T(8,128)(2,1)S(1)}, u32[]{:S(2)}) copy-start(bf16[256,1024]{1,0:T(8,128)(2,1)S(1)} %collective-permute-done.1.refs_2_) | copy-start | bytes 1572868
  16.7 11.3 %collective-permute-start.2 = (bf16[256,1024]{1,0:T(8,128)(2,1)S(1)}, bf16[256,1024]{1,0:T(8,128)(2,1)S(1)}, u32[]{:S(2)}, u32[]{:S(2)}) collective-permute-start(bf16[256,1024]{1,0:T(8,128)(2,1)S(1)} %collective-permute-done.1.refs_2_), channel_id=1, source_target_pairs={{0,1},{1,0},{2,3},{3,2},{4,5},{5,4},{6,7},{7,6},{8,9},{9,8},{10,11... | collective-permute-start | bytes 1572872 | tf_op jit(solution)/shard_map/ppermute | solution.py:40
  16.7 27.0 %collective-permute-start.3 = (bf16[256,1024]{1,0:T(8,128)(2,1)}, bf16[256,1024]{1,0:T(8,128)(2,1)S(1)}, u32[]{:S(2)}, u32[]{:S(2)}) collective-permute-start(bf16[256,1024]{1,0:T(8,128)(2,1)} %refs_4_.1), channel_id=1, source_target_pairs={{0,1},{1,0},{2,3},{3,2},{4,5},{5,4},{6,7},{7,6},{8,9},{9,8},{10,11... | collective-permute-start | bytes 1572872 | tf_op jit(solution)/shard_map/ppermute | solution.py:40
  27.0 16.6 %copy-start.3 = (bf16[256,1024]{1,0:T(8,128)(2,1)}, bf16[256,1024]{1,0:T(8,128)(2,1)S(1)}, u32[]{:S(2)}) copy-start(bf16[256,1024]{1,0:T(8,128)(2,1)S(1)} %collective-permute-done.4.refs_6_) | copy-start | bytes 1572868
  27.0 16.7 %collective-permute-start.5 = (bf16[256,1024]{1,0:T(8,128)(2,1)S(1)}, bf16[256,1024]{1,0:T(8,128)(2,1)S(1)}, u32[]{:S(2)}, u32[]{:S(2)}) collective-permute-start(bf16[256,1024]{1,0:T(8,128)(2,1)S(1)} %collective-permute-done.4.refs_6_), channel_id=1, source_target_pairs={{0,1},{1,0},{2,3},{3,2},{4,5},{5,4},{6,7},{7,6},{8,9},{9,8},{10,11... | collective-permute-start | bytes 1572872 | tf_op jit(solution)/shard_map/ppermute | solution.py:40
  28.0 1.0 copy-start.5
  43.7 0.8 copy-start.6
  43.7 1.0 copy-start.7
  57.8 42.6 %collective-permute-start.8 = (bf16[2,528,256]{2,1,0:T(8,128)(2,1)}, bf16[2,528,256]{2,1,0:T(8,128)(2,1)S(1)}, u32[]{:S(2)}, u32[]{:S(2)}) collective-permute-start(bf16[2,528,256]{2,1,0:T(8,128)(2,1)} %get-tuple-element.58), channel_id=1, source_target_pairs={{0,4},{4,0},{8,12},{12,8},{16,20},{20,16},{24,28},{28,24},{1,5},{5... | collective-permute-start | bytes 1622024 | tf_op jit(solution)/shard_map/ppermute | solution.py:40
  59.7 13.2 %copy-start.15 = (f32[6,352]{1,0:T(8,128)S(1)}, f32[6,352]{1,0:T(8,128)}, u32[]{:S(2)}) copy-start(f32[6,352]{1,0:T(8,128)} %get-tuple-element.81) | copy-start | bytes 25348
  73.7 8.7 %collective-permute-start.28 = (f32[6,704]{1,0:T(8,128)S(1)}, f32[6,704]{1,0:T(8,128)S(1)}, u32[]{:S(2)}, u32[]{:S(2)}) collective-permute-start(f32[6,704]{1,0:T(8,128)S(1)} %pad_maximum_fusion.4), channel_id=1, source_target_pairs={{0,4},{4,0},{8,12},{12,8},{16,20},{20,16},{24,28},{28,24},{1,5},{5... | collective-permute-start | bytes 50696 | tf_op jit(solution)/shard_map/ppermute | solution.py:40
  74.0 29.4 %collective-permute-start.13 = (bf16[2,528,256]{2,1,0:T(8,128)(2,1)}, bf16[2,528,256]{2,1,0:T(8,128)(2,1)S(1)}, u32[]{:S(2)}, u32[]{:S(2)}) collective-permute-start(bf16[2,528,256]{2,1,0:T(8,128)(2,1)} %get-tuple-element.60), channel_id=1, source_target_pairs={{0,8},{4,12},{8,0},{12,4},{16,24},{20,28},{24,16},{28,20},{1,9},{5... | collective-permute-start | bytes 1622024 | tf_op jit(solution)/shard_map/ppermute | solution.py:40
  75.8 29.3 %collective-permute-start.18 = (bf16[2,528,256]{2,1,0:T(8,128)(2,1)}, bf16[2,528,256]{2,1,0:T(8,128)(2,1)S(1)}, u32[]{:S(2)}, u32[]{:S(2)}) collective-permute-start(bf16[2,528,256]{2,1,0:T(8,128)(2,1)} %get-tuple-element.62), channel_id=1, source_target_pairs={{0,8},{4,12},{8,0},{12,4},{16,24},{20,28},{24,16},{28,20},{1,9},{5... | collective-permute-start | bytes 1622024 | tf_op jit(solution)/shard_map/ppermute | solution.py:40
  76.0 6.4 %copy-start.16 = (f32[6,352]{1,0:T(8,128)S(1)}, f32[6,352]{1,0:T(8,128)}, u32[]{:S(2)}) copy-start(f32[6,352]{1,0:T(8,128)} %get-tuple-element.80) | copy-start | bytes 25348
  82.5 8.4 %copy-start.17 = (bf16[2,528,256]{2,1,0:T(8,128)(2,1)S(1)}, bf16[2,528,256]{2,1,0:T(8,128)(2,1)}, u32[]{:S(2)}) copy-start(bf16[2,528,256]{2,1,0:T(8,128)(2,1)} %get-tuple-element.64) | copy-start | bytes 1622020
  82.5 17.9 %copy-start.10 = (bf16[2,256,1024]{2,1,0:T(8,128)(2,1)S(1)}, bf16[2,256,1024]{2,1,0:T(8,128)(2,1)}, u32[]{:S(2)}) copy-start(bf16[2,256,1024]{2,1,0:T(8,128)(2,1)} %input_part.3) | copy-start | bytes 3145732
  82.5 20.7 %copy-start.14 = (bf16[2,528,256]{2,1,0:T(8,128)(2,1)S(1)}, bf16[2,528,256]{2,1,0:T(8,128)(2,1)}, u32[]{:S(2)}) copy-start(bf16[2,528,256]{2,1,0:T(8,128)(2,1)} %get-tuple-element.57) | copy-start | bytes 1622020
  82.5 22.5 %copy-start.12 = (bf16[2,528,256]{2,1,0:T(8,128)(2,1)S(1)}, bf16[2,528,256]{2,1,0:T(8,128)(2,1)}, u32[]{:S(2)}) copy-start(bf16[2,528,256]{2,1,0:T(8,128)(2,1)} %get-tuple-element.59) | copy-start | bytes 1622020
  82.5 24.1 %copy-start.13 = (bf16[2,528,256]{2,1,0:T(8,128)(2,1)S(1)}, bf16[2,528,256]{2,1,0:T(8,128)(2,1)}, u32[]{:S(2)}) copy-start(bf16[2,528,256]{2,1,0:T(8,128)(2,1)} %get-tuple-element.61) | copy-start | bytes 1622020
  82.5 24.8 %copy-start.11 = (bf16[2,528,256]{2,1,0:T(8,128)(2,1)S(1)}, bf16[2,528,256]{2,1,0:T(8,128)(2,1)}, u32[]{:S(2)}) copy-start(bf16[2,528,256]{2,1,0:T(8,128)(2,1)} %get-tuple-element.63) | copy-start | bytes 1622020
  82.5 17.9 %collective-permute-start.29 = (f32[6,704]{1,0:T(8,128)S(1)}, f32[6,704]{1,0:T(8,128)S(1)}, u32[]{:S(2)}, u32[]{:S(2)}) collective-permute-start(f32[6,704]{1,0:T(8,128)S(1)} %fusion.12), channel_id=1, source_target_pairs={{0,8},{4,12},{8,0},{12,4},{16,24},{20,28},{24,16},{28,20},{1,9},{5... | collective-permute-start | bytes 50696 | tf_op jit(solution)/shard_map/ppermute | solution.py:40
  90.9 15.8 %collective-permute-start.23 = (bf16[2,528,256]{2,1,0:T(8,128)(2,1)S(1)}, bf16[2,528,256]{2,1,0:T(8,128)(2,1)S(1)}, u32[]{:S(2)}, u32[]{:S(2)}) collective-permute-start(bf16[2,528,256]{2,1,0:T(8,128)(2,1)S(1)} %copy-done.17), channel_id=1, source_target_pairs={{0,4},{4,0},{8,12},{12,8},{16,20},{20,16},{24,28},{28,24},{1,5},{5... | collective-permute-start | bytes 1622024 | tf_op jit(solution)/shard_map/ppermute | solution.py:40
  100.4 25.5 %collective-permute-start.6 = (bf16[2,256,1024]{2,1,0:T(8,128)(2,1)S(1)}, bf16[2,256,1024]{2,1,0:T(8,128)(2,1)S(1)}, u32[]{:S(2)}, u32[]{:S(2)}) collective-permute-start(bf16[2,256,1024]{2,1,0:T(8,128)(2,1)S(1)} %copy-done.10), channel_id=1, source_target_pairs={{0,1},{1,0},{2,3},{3,2},{4,5},{5,4},{6,7},{7,6},{8,9},{9,8},{10,11... | collective-permute-start | bytes 3145736 | tf_op jit(solution)/shard_map/ppermute | solution.py:40
  100.4 77.5 %collective-permute-start.30 = (f32[6,704]{1,0:T(8,128)S(1)}, f32[6,704]{1,0:T(8,128)S(1)}, u32[]{:S(2)}, u32[]{:S(2)}) collective-permute-start(f32[6,704]{1,0:T(8,128)S(1)} %add.117), channel_id=1, source_target_pairs={{0,16},{4,20},{8,24},{12,28},{16,0},{20,4},{24,8},{28,12},{1,17},{... | collective-permute-start | bytes 50696 | tf_op jit(solution)/shard_map/ppermute | solution.py:40
  103.3 8.7 %collective-permute-start.9 = (bf16[528,256]{1,0:T(8,128)(2,1)S(1)}, bf16[528,256]{1,0:T(8,128)(2,1)S(1)}, u32[]{:S(2)}, u32[]{:S(2)}) collective-permute-start(bf16[528,256]{1,0:T(8,128)(2,1)S(1)} %fusion.8), channel_id=1, source_target_pairs={{0,8},{4,12},{8,0},{12,4},{16,24},{20,28},{24,16},{28,20},{1,9},{5... | collective-permute-start | bytes 811016 | tf_op jit(solution)/shard_map/ppermute | solution.py:40
  105.0 9.4 %collective-permute-start.14 = (bf16[528,256]{1,0:T(8,128)(2,1)S(1)}, bf16[528,256]{1,0:T(8,128)(2,1)S(1)}, u32[]{:S(2)}, u32[]{:S(2)}) collective-permute-start(bf16[528,256]{1,0:T(8,128)(2,1)S(1)} %fusion.9), channel_id=1, source_target_pairs={{0,4},{4,0},{8,12},{12,8},{16,20},{20,16},{24,28},{28,24},{1,5},{5... | collective-permute-start | bytes 811016 | tf_op jit(solution)/shard_map/ppermute | solution.py:40
  106.6 20.0 %copy-start.1 = (f32[2,256,1024]{2,1,0:T(8,128)S(1)}, f32[2,256,1024]{2,1,0:T(8,128)}, u32[]{:S(2)}) copy-start(f32[2,256,1024]{2,1,0:T(8,128)} %input_part.2) | copy-start | bytes 6291460
  106.7 12.5 %collective-permute-start.19 = (bf16[528,256]{1,0:T(8,128)(2,1)S(1)}, bf16[528,256]{1,0:T(8,128)(2,1)S(1)}, u32[]{:S(2)}, u32[]{:S(2)}) collective-permute-start(bf16[528,256]{1,0:T(8,128)(2,1)S(1)} %fusion.10), channel_id=1, source_target_pairs={{0,4},{4,0},{8,12},{12,8},{16,20},{20,16},{24,28},{28,24},{1,5},{5... | collective-permute-start | bytes 811016 | tf_op jit(solution)/shard_map/ppermute | solution.py:40
  112.0 11.5 %collective-permute-start.24 = (bf16[528,256]{1,0:T(8,128)(2,1)S(1)}, bf16[528,256]{1,0:T(8,128)(2,1)S(1)}, u32[]{:S(2)}, u32[]{:S(2)}) collective-permute-start(bf16[528,256]{1,0:T(8,128)(2,1)S(1)} %fusion.11), channel_id=1, source_target_pairs={{0,8},{4,12},{8,0},{12,4},{16,24},{20,28},{24,16},{28,20},{1,9},{5... | collective-permute-start | bytes 811016 | tf_op jit(solution)/shard_map/ppermute | solution.py:40
  114.5 32.9 %collective-permute-start.10 = (bf16[528,256]{1,0:T(8,128)(2,1)S(1)}, bf16[528,256]{1,0:T(8,128)(2,1)S(1)}, u32[]{:S(2)}, u32[]{:S(2)}) collective-permute-start(bf16[528,256]{1,0:T(8,128)(2,1)S(1)} %fusion.6), channel_id=1, source_target_pairs={{0,16},{4,20},{8,24},{12,28},{16,0},{20,4},{24,8},{28,12},{1,17},{... | collective-permute-start | bytes 811016 | tf_op jit(solution)/shard_map/ppermute | solution.py:40
  119.2 34.1 %collective-permute-start.15 = (bf16[528,256]{1,0:T(8,128)(2,1)S(1)}, bf16[528,256]{1,0:T(8,128)(2,1)S(1)}, u32[]{:S(2)}, u32[]{:S(2)}) collective-permute-start(bf16[528,256]{1,0:T(8,128)(2,1)S(1)} %fusion.5), channel_id=1, source_target_pairs={{0,16},{4,20},{8,24},{12,28},{16,0},{20,4},{24,8},{28,12},{1,17},{... | collective-permute-start | bytes 811016 | tf_op jit(solution)/shard_map/ppermute | solution.py:40
  123.5 35.6 %collective-permute-start.20 = (bf16[528,256]{1,0:T(8,128)(2,1)S(1)}, bf16[528,256]{1,0:T(8,128)(2,1)S(1)}, u32[]{:S(2)}, u32[]{:S(2)}) collective-permute-start(bf16[528,256]{1,0:T(8,128)(2,1)S(1)} %fusion.4), channel_id=1, source_target_pairs={{0,16},{4,20},{8,24},{12,28},{16,0},{20,4},{24,8},{28,12},{1,17},{... | collective-permute-start | bytes 811016 | tf_op jit(solution)/shard_map/ppermute | solution.py:40
  125.9 36.9 %collective-permute-start.25 = (bf16[528,256]{1,0:T(8,128)(2,1)S(1)}, bf16[528,256]{1,0:T(8,128)(2,1)S(1)}, u32[]{:S(2)}, u32[]{:S(2)}) collective-permute-start(bf16[528,256]{1,0:T(8,128)(2,1)S(1)} %fusion.3), channel_id=1, source_target_pairs={{0,16},{4,20},{8,24},{12,28},{16,0},{20,4},{24,8},{28,12},{1,17},{... | collective-permute-start | bytes 811016 | tf_op jit(solution)/shard_map/ppermute | solution.py:40
  147.4 32.7 %collective-permute-start.7 = (bf16[1,256,1024]{2,1,0:T(8,128)(2,1)S(1)}, bf16[1,256,1024]{2,1,0:T(8,128)(2,1)S(1)}, u32[]{:S(2)}, u32[]{:S(2)}) collective-permute-start(bf16[1,256,1024]{2,1,0:T(8,128)(2,1)S(1)} %fusion), channel_id=1, source_target_pairs={{0,2},{2,0},{1,3},{3,1},{4,6},{6,4},{5,7},{7,5},{8,10},{10,8},{9,1... | collective-permute-start | bytes 1572872 | tf_op jit(solution)/shard_map/ppermute | solution.py:40
  153.3 15.2 %collective-permute-start.11 = (bf16[528,256]{1,0:T(8,128)(2,1)S(1)}, bf16[528,256]{1,0:T(8,128)(2,1)S(1)}, u32[]{:S(2)}, u32[]{:S(2)}) collective-permute-start(bf16[528,256]{1,0:T(8,128)(2,1)S(1)} %add_convert_fusion.6), channel_id=1, source_target_pairs={{0,8},{4,12},{8,0},{12,4},{16,24},{20,28},{24,16},{28,20},{1,9},{5... | collective-permute-start | bytes 811016 | tf_op jit(solution)/shard_map/ppermute | solution.py:40
  159.1 9.5 %collective-permute-start.16 = (bf16[528,256]{1,0:T(8,128)(2,1)S(1)}, bf16[528,256]{1,0:T(8,128)(2,1)S(1)}, u32[]{:S(2)}, u32[]{:S(2)}) collective-permute-start(bf16[528,256]{1,0:T(8,128)(2,1)S(1)} %add_convert_fusion.4), channel_id=1, source_target_pairs={{0,4},{4,0},{8,12},{12,8},{16,20},{20,16},{24,28},{28,24},{1,5},{5... | collective-permute-start | bytes 811016 | tf_op jit(solution)/shard_map/ppermute | solution.py:40
  162.8 8.6 %collective-permute-start.21 = (bf16[528,256]{1,0:T(8,128)(2,1)S(1)}, bf16[528,256]{1,0:T(8,128)(2,1)S(1)}, u32[]{:S(2)}, u32[]{:S(2)}) collective-permute-start(bf16[528,256]{1,0:T(8,128)(2,1)S(1)} %add_convert_fusion.2), channel_id=1, source_target_pairs={{0,4},{4,0},{8,12},{12,8},{16,20},{20,16},{24,28},{28,24},{1,5},{5... | collective-permute-start | bytes 811016 | tf_op jit(solution)/shard_map/ppermute | solution.py:40
  168.5 9.4 %collective-permute-start.26 = (bf16[528,256]{1,0:T(8,128)(2,1)S(1)}, bf16[528,256]{1,0:T(8,128)(2,1)S(1)}, u32[]{:S(2)}, u32[]{:S(2)}) collective-permute-start(bf16[528,256]{1,0:T(8,128)(2,1)S(1)} %add_convert_fusion), channel_id=1, source_target_pairs={{0,8},{4,12},{8,0},{12,4},{16,24},{20,28},{24,16},{28,20},{1,9},{5... | collective-permute-start | bytes 811016 | tf_op jit(solution)/shard_map/ppermute | solution.py:40
  168.6 37.1 %collective-permute-start.12 = (bf16[2,528,256]{2,1,0:T(8,128)(2,1)S(1)}, bf16[2,528,256]{2,1,0:T(8,128)(2,1)S(1)}, u32[]{:S(2)}, u32[]{:S(2)}) collective-permute-start(bf16[2,528,256]{2,1,0:T(8,128)(2,1)S(1)} %pad_maximum_fusion.refs_0_), channel_id=1, source_target_pairs={{0,4},{4,0},{8,12},{12,8},{16,20},{20,16},{24,28},{28,24},{1,5},{5... | collective-permute-start | bytes 1622024 | tf_op jit(solution)/shard_map/ppermute | solution.py:40
  170.2 24.3 %copy-start = (s32[2]{0:T(128)S(1)}, s32[2]{0:T(128)}, u32[]{:S(2)}) copy-start(s32[2]{0:T(128)} %pad_add_fusion.me_ref.where_ref) | copy-start | bytes 28
  171.4 32.3 %collective-permute-start.17 = (bf16[2,528,256]{2,1,0:T(8,128)(2,1)S(1)}, bf16[2,528,256]{2,1,0:T(8,128)(2,1)S(1)}, u32[]{:S(2)}, u32[]{:S(2)}) collective-permute-start(bf16[2,528,256]{2,1,0:T(8,128)(2,1)S(1)} %pad_maximum_fusion.1.refs_0_), channel_id=1, source_target_pairs={{0,8},{4,12},{8,0},{12,4},{16,24},{20,28},{24,16},{28,20},{1,9},{5... | collective-permute-start | bytes 1622024 | tf_op jit(solution)/shard_map/ppermute | solution.py:40
  177.9 22.2 %collective-permute-start.22 = (bf16[2,528,256]{2,1,0:T(8,128)(2,1)S(1)}, bf16[2,528,256]{2,1,0:T(8,128)(2,1)S(1)}, u32[]{:S(2)}, u32[]{:S(2)}) collective-permute-start(bf16[2,528,256]{2,1,0:T(8,128)(2,1)S(1)} %pad_maximum_fusion.2.refs_0_), channel_id=1, source_target_pairs={{0,8},{4,12},{8,0},{12,4},{16,24},{20,28},{24,16},{28,20},{1,9},{5... | collective-permute-start | bytes 1622024 | tf_op jit(solution)/shard_map/ppermute | solution.py:40
  178.0 16.6 %collective-permute-start.27 = (bf16[2,528,256]{2,1,0:T(8,128)(2,1)S(1)}, bf16[2,528,256]{2,1,0:T(8,128)(2,1)S(1)}, u32[]{:S(2)}, u32[]{:S(2)}) collective-permute-start(bf16[2,528,256]{2,1,0:T(8,128)(2,1)S(1)} %pad_maximum_fusion.3.refs_0_), channel_id=1, source_target_pairs={{0,4},{4,0},{8,12},{12,8},{16,20},{20,16},{24,28},{28,24},{1,5},{5... | collective-permute-start | bytes 1622024 | tf_op jit(solution)/shard_map/ppermute | solution.py:40
  (1 other events, 0.8 us)

commit v3 on v2

--- a/solution.py
+++ b/solution.py
@@ -44,8 +44,8 @@
     (0, (0, 1)),
     (1, (0, 1)),
     (2, (0,)),
+    (2, (1,)),
     (3, (0, 1)),
-    (2, (1,)),
 )
 
 
@@ -203,7 +203,7 @@
         low = start - offset
         down_ref, hidden_ref, silu_ref, slope_ref, upg_ref, upv_ref = [buf.at[low : low + height] for buf in bufs]
         ggrad_ref, vgrad_ref = [grad.at[low : low + height] for grad in grads]
-        gtaps, vtaps = gtaps_ref.at[low : low + height], vtaps_ref.at[low : low + height]
+        gtaps, vtaps = gtaps_ref.at[start : start + height], vtaps_ref.at[start : start + height]
         arrived((g, 0))
         for r, (at, piece) in enumerate(zip(spots, cots)):
             if g == 0:
@@ -283,14 +283,12 @@
     parts, rows = len(toks), toks[0].shape[0]
     tokens, count = parts * rows, gtaps.shape[1]
     height, most = sum(group[1] for group in groups), max(group[1] for group in groups)
-    offset = groups[0][0]
     payloads = [(2, 3 * part, model // 4) for group in groups for part in group[2] for _ in range(2)]
     anywhere = pl.BlockSpec(memory_space=pl.ANY)
     vmem = pl.BlockSpec(memory_space=pltpu.VMEM)
     sums = [(2 * count, group[1]) for group in groups]
     shapes = (*payloads, (height, tokens), (height, tokens), *sums)
     types = (BF16,) * (len(payloads) + 2) + (F32,) * len(sums)
-    mine = slice(offset, offset + height)
     return pl.pallas_call(
         functools.partial(backward_kernel, parts, groups),
         out_shape=tuple(jax.ShapeDtypeStruct(s, t) for s, t in zip(shapes, types)),
@@ -316,7 +314,7 @@
             flops=8 * height * tokens * model, bytes_accessed=8 * tokens * model, transcendentals=0
         ),
         name="backward_part",
-    )(me, *toks, *cots, down, hidden, silu, slope, upg, upv, gtaps[mine], vtaps[mine])
+    )(me, *toks, *cots, down, hidden, silu, slope, upg, upv, gtaps, vtaps)
 
 
 def input_kernel(me_ref, *refs):

time: 208 us -> 201 us (0.966)
  waiting for transfers between devices: 102 us -> 93.2 us
    ppermute x31, waiting for transfers between devices: 102 us -> 93.2 us  [exchange(): return lax.ppermute(value, axis, [(i, i ^ 1 << bit) for i in range(size)])]
    unnamed x38 -> x34, local copies, waits for them, and re-layouts: 3.82 us -> 5.3 us
  transfers between devices with their start and end apart: 31 -> 31, of which waited for: 16 -> 14; matrix products, arithmetic and copies ran while one was open for 4% -> 4% of each run, Pallas kernels for 23% -> 24%
where the time goes in v3:
time: 201 us; the launch traced here: 200 us
  waiting for transfers between devices  93.2 us (46%)
  Pallas kernels  63 us (31%)
  starting transfers between devices  33.2 us (17%)
  local copies, waits for them, and re-layouts  5.92 us (3%)
  other arithmetic  3.88 us (2%)
    ppermute x31, waiting for transfers between devices, exchange(): return lax.ppermute(value, axis, [(i, i ^ 1 << bit) for i in range(size)])  93.2 us
    ppermute x31, starting transfers between devices, exchange(): return lax.ppermute(value, axis, [(i, i ^ 1 << bit) for i in range(size)])  33.2 us
    pallas_call x2, Pallas kernels, backward_part(): pl.pallas_call(functools.partial(backward_kernel, parts, groups), out_sha...  26.3 us
    pallas_call x1, Pallas kernels, forward_part(): pl.pallas_call(functools.partial(forward_kernel, parts), out_shape=tuple(...  14.7 us
    pallas_call x2, Pallas kernels, input_part(): pl.pallas_call(input_kernel, out_shape=jax.ShapeDtypeStruct((half, rows,...  12.9 us
    pallas_call x5, Pallas kernels, place(): pl.pallas_call(functools.partial(place_kernel, scale, start, sides, swap,...  9.11 us
    unnamed x34, local copies, waits for them, and re-layouts  5.3 us
  transfers between devices with their start and end apart: 31, of which 14 were waited for; matrix products, arithmetic and copies ran while one was open for 4% of the time, Pallas kernels for 24%

profile of v3, /device:TPU:0, one launch (start us, length us, event | category | flops | bytes accessed | tf_op | source)
XLA Modules:
  0.0 200.3 jit_solution(17034195613870922915)
XLA Ops:
  0.6 3.0 %collective-permute-start.1 = (bf16[256,1024]{1,0:T(8,128)(2,1)}, bf16[256,1024]{1,0:T(8,128)(2,1)S(1)}, u32[]{:S(2)}, u32[]{:S(2)}) collective-permute-start(bf16[256,1024]{1,0:T(8,128)(2,1)} %refs_0_.5), channel_id=1, source_target_pairs={{0,2},{2,0},{1,3},{3,1},{4,6},{6,4},{5,7},{7,5},{8,10},{10,8},{9,1... | collective-permute-start | bytes 1572872 | tf_op jit(solution)/shard_map/ppermute | solution.py:40
  3.7 1.6 copy.25
  5.3 1.6 copy.26
  6.9 0.6 pad_add_fusion.me_ref.where_ref
  7.5 9.1 %collective-permute-done.1.refs_2_ = bf16[256,1024]{1,0:T(8,128)(2,1)S(1)} collective-permute-done((bf16[256,1024]{1,0:T(8,128)(2,1)}, bf16[256,1024]{1,0:T(8,128)(2,1)S(1)}, u32[]{:S(2)}, u32[]{:S(2)}) %collective-permute-start.1) | collective-permute-done | bytes 524320 | tf_op jit(solution)/shard_map/ppermute | solution.py:40
  17.2 9.9 %collective-permute-done.4.refs_6_ = bf16[256,1024]{1,0:T(8,128)(2,1)S(1)} collective-permute-done((bf16[256,1024]{1,0:T(8,128)(2,1)}, bf16[256,1024]{1,0:T(8,128)(2,1)S(1)}, u32[]{:S(2)}, u32[]{:S(2)}) %collective-permute-start.4) | collective-permute-done | bytes 524320 | tf_op jit(solution)/shard_map/ppermute | solution.py:40
  27.1 0.8 copy-done.4
  28.1 14.7 %forward_part.1 = (bf16[704,1024]{1,0:T(8,128)(2,1)}, f32[704,1024]{1,0:T(8,128)}, f32[704,1024]{1,0:T(8,128)}, bf16[704,1024]{1,0:T(8,128)(2,1)}, bf16[704,1024]{1,0:T(8,128)(2,1)}) custom-call(s32[2]{0:T(128)} %pad_add_fusion.me_ref.where_ref, bf16[256,1024]{1,0:T(8,128)(2,1)} %refs_0_.5, bf16[256,1024]{1,0:T(8,128)(2,1)} %copy-done.4, ...), custom_call_target="tpu_custom_call" | custom-call | flops 2952790016 | bytes 12976128 | tf_op jit(solution)/shard_map/forward_part/pallas_call | solution.py:141
  42.8 0.8 copy-done.6
  43.8 13.2 %backward_part.3 = (bf16[2,528,256]{2,1,0:T(8,128)(2,1)}, bf16[2,528,256]{2,1,0:T(8,128)(2,1)}, bf16[2,528,256]{2,1,0:T(8,128)(2,1)}, bf16[2,528,256]{2,1,0:T(8,...) custom-call(s32[2]{0:T(128)} %pad_add_fusion.me_ref.where_ref, ...), custom_call_target="tpu_custom_call" | custom-call | flops 2952790016 | bytes 8388608 | tf_op jit(solution)/shard_map/backward_part/pallas_call | solution.py:292
  57.0 1.9 collective-permute-start.8
  58.9 13.2 %backward_part.2 = (bf16[2,528,256]{2,1,0:T(8,128)(2,1)}, bf16[2,528,256]{2,1,0:T(8,128)(2,1)}, bf16[2,528,256]{2,1,0:T(8,128)(2,1)}, bf16[2,528,256]{2,1,0:T(8,...) custom-call(s32[2]{0:T(128)} %pad_add_fusion.me_ref.where_ref, ...), custom_call_target="tpu_custom_call" | custom-call | flops 2952790016 | bytes 8388608 | tf_op jit(solution)/shard_map/backward_part/pallas_call | solution.py:292
  72.1 0.8 pad_maximum_fusion.4
  72.9 1.5 collective-permute-start.28
  75.1 6.4 %input_part.3 = bf16[2,256,1024]{2,1,0:T(8,128)(2,1)} custom-call(s32[2]{0:T(128)} %pad_add_fusion.me_ref.where_ref, bf16[352,1024]{1,0:T(8,128)(2,1)} %get-tuple-element.53.refs_0_, bf16[352,1024]{1,0:T(8,128)(2,1)} %get-tuple-element.54.refs_1_, bf16[352,1024]{1,0:T(8,128)(2,1)} %get-tuple-element.55.refs_2_, bf16[352,1024]{1,0:T(8,128)(2,1)} %get-tuple-element.56.refs_3_, ...), custom_call_target="tpu_custom_call" | custom-call | flops 1476395008 | bytes 4587520 | tf_op jit(solution)/shard_map/input_part/pallas_call | solution.py:343
  81.6 1.9 collective-permute-start.29
  83.5 6.5 %input_part.2 = f32[2,256,1024]{2,1,0:T(8,128)} custom-call(s32[2]{0:T(128)} %pad_add_fusion.me_ref.where_ref, bf16[352,1024]{1,0:T(8,128)(2,1)} %get-tuple-element.53.refs_0_, bf16[352,1024]{1,0:T(8,128)(2,1)} %get-tuple-element.54.refs_1_, bf16[352,1024]{1,0:T(8,128)(2,1)} %get-tuple-element.55.refs_2_, bf16[352,1024]{1,0:T(8,128)(2,1)} %get-tuple-element.56.refs_3_, ...), custom_call_target="tpu_custom_call" | custom-call | flops 1476395008 | bytes 4587520 | tf_op jit(solution)/shard_map/input_part/pallas_call | solution.py:343
  90.0 1.6 collective-permute-start.23
  91.6 2.7 %collective-permute-start.30 = (f32[6,704]{1,0:T(8,128)S(1)}, f32[6,704]{1,0:T(8,128)S(1)}, u32[]{:S(2)}, u32[]{:S(2)}) collective-permute-start(f32[6,704]{1,0:T(8,128)S(1)} %add.117), channel_id=1, source_target_pairs={{0,16},{4,20},{8,24},{12,28},{16,0},{20,4},{24,8},{28,12},{1,17},{... | collective-permute-start | bytes 50696 | tf_op jit(solution)/shard_map/ppermute | solution.py:40
  95.0 0.7 collective-permute-start.14
  95.7 9.5 %collective-permute-done.23 = bf16[2,528,256]{2,1,0:T(8,128)(2,1)S(1)} collective-permute-done((bf16[2,528,256]{2,1,0:T(8,128)(2,1)S(1)}, bf16[2,528,256]{2,1,0:T(8,128)(2,1)S(1)}, u32[]{:S(2)}, u32[]{:S(2)}) %collective-permute-start.23) | collective-permute-done | bytes 540704 | tf_op jit(solution)/shard_map/ppermute | solution.py:40
  105.2 1.5 collective-permute-start.19
  106.8 4.2 %collective-permute-done.9 = bf16[528,256]{1,0:T(8,128)(2,1)S(1)} collective-permute-done((bf16[528,256]{1,0:T(8,128)(2,1)S(1)}, bf16[528,256]{1,0:T(8,128)(2,1)S(1)}, u32[]{:S(2)}, u32[]{:S(2)}) %collective-permute-start.9) | collective-permute-done | bytes 270368 | tf_op jit(solution)/shard_map/ppermute | solution.py:40
  111.5 2.9 %collective-permute-start.10 = (bf16[528,256]{1,0:T(8,128)(2,1)S(1)}, bf16[528,256]{1,0:T(8,128)(2,1)S(1)}, u32[]{:S(2)}, u32[]{:S(2)}) collective-permute-start(bf16[528,256]{1,0:T(8,128)(2,1)S(1)} %fusion.6), channel_id=1, source_target_pairs={{0,16},{4,20},{8,24},{12,28},{16,0},{20,4},{24,8},{28,12},{1,17},{... | collective-permute-start | bytes 811016 | tf_op jit(solution)/shard_map/ppermute | solution.py:40
  114.9 2.6 %collective-permute-start.15 = (bf16[528,256]{1,0:T(8,128)(2,1)S(1)}, bf16[528,256]{1,0:T(8,128)(2,1)S(1)}, u32[]{:S(2)}, u32[]{:S(2)}) collective-permute-start(bf16[528,256]{1,0:T(8,128)(2,1)S(1)} %fusion.5), channel_id=1, source_target_pairs={{0,16},{4,20},{8,24},{12,28},{16,0},{20,4},{24,8},{28,12},{1,17},{... | collective-permute-start | bytes 811016 | tf_op jit(solution)/shard_map/ppermute | solution.py:40
  117.6 2.9 %collective-permute-done.24 = bf16[528,256]{1,0:T(8,128)(2,1)S(1)} collective-permute-done((bf16[528,256]{1,0:T(8,128)(2,1)S(1)}, bf16[528,256]{1,0:T(8,128)(2,1)S(1)}, u32[]{:S(2)}, u32[]{:S(2)}) %collective-permute-start.24) | collective-permute-done | bytes 270368 | tf_op jit(solution)/shard_map/ppermute | solution.py:40
  120.5 2.4 %collective-permute-start.20 = (bf16[528,256]{1,0:T(8,128)(2,1)S(1)}, bf16[528,256]{1,0:T(8,128)(2,1)S(1)}, u32[]{:S(2)}, u32[]{:S(2)}) collective-permute-start(bf16[528,256]{1,0:T(8,128)(2,1)S(1)} %fusion.4), channel_id=1, source_target_pairs={{0,16},{4,20},{8,24},{12,28},{16,0},{20,4},{24,8},{28,12},{1,17},{... | collective-permute-start | bytes 811016 | tf_op jit(solution)/shard_map/ppermute | solution.py:40
  123.0 0.6 collective-permute-start.25
  123.8 19.9 %collective-permute-done.10 = bf16[528,256]{1,0:T(8,128)(2,1)S(1)} collective-permute-done((bf16[528,256]{1,0:T(8,128)(2,1)S(1)}, bf16[528,256]{1,0:T(8,128)(2,1)S(1)}, u32[]{:S(2)}, u32[]{:S(2)}) %collective-permute-start.10) | collective-permute-done | bytes 270368 | tf_op jit(solution)/shard_map/ppermute | solution.py:40
  143.7 1.5 collective-permute-start.7
  145.3 4.2 %collective-permute-done.15 = bf16[528,256]{1,0:T(8,128)(2,1)S(1)} collective-permute-done((bf16[528,256]{1,0:T(8,128)(2,1)S(1)}, bf16[528,256]{1,0:T(8,128)(2,1)S(1)}, u32[]{:S(2)}, u32[]{:S(2)}) %collective-permute-start.15) | collective-permute-done | bytes 270368 | tf_op jit(solution)/shard_map/ppermute | solution.py:40
  149.5 1.5 collective-permute-start.11
  151.1 4.3 %collective-permute-done.20 = bf16[528,256]{1,0:T(8,128)(2,1)S(1)} collective-permute-done((bf16[528,256]{1,0:T(8,128)(2,1)S(1)}, bf16[528,256]{1,0:T(8,128)(2,1)S(1)}, u32[]{:S(2)}, u32[]{:S(2)}) %collective-permute-start.20) | collective-permute-done | bytes 270368 | tf_op jit(solution)/shard_map/ppermute | solution.py:40
  155.5 2.9 %collective-permute-done.25 = bf16[528,256]{1,0:T(8,128)(2,1)S(1)} collective-permute-done((bf16[528,256]{1,0:T(8,128)(2,1)S(1)}, bf16[528,256]{1,0:T(8,128)(2,1)S(1)}, u32[]{:S(2)}, u32[]{:S(2)}) %collective-permute-start.25) | collective-permute-done | bytes 270368 | tf_op jit(solution)/shard_map/ppermute | solution.py:40
  158.3 1.5 collective-permute-start.21
  160.1 4.7 %collective-permute-done.16 = bf16[528,256]{1,0:T(8,128)(2,1)S(1)} collective-permute-done((bf16[528,256]{1,0:T(8,128)(2,1)S(1)}, bf16[528,256]{1,0:T(8,128)(2,1)S(1)}, u32[]{:S(2)}, u32[]{:S(2)}) %collective-permute-start.16) | collective-permute-done | bytes 270368 | tf_op jit(solution)/shard_map/ppermute | solution.py:40
  164.8 1.6 collective-permute-start.17
  166.4 4.1 %collective-permute-done.26 = bf16[528,256]{1,0:T(8,128)(2,1)S(1)} collective-permute-done((bf16[528,256]{1,0:T(8,128)(2,1)S(1)}, bf16[528,256]{1,0:T(8,128)(2,1)S(1)}, u32[]{:S(2)}, u32[]{:S(2)}) %collective-permute-start.26) | collective-permute-done | bytes 270368 | tf_op jit(solution)/shard_map/ppermute | solution.py:40
  170.6 1.6 collective-permute-start.27
  172.2 0.6 fusion.13
  172.8 1.0 fusion.7
  173.9 15.5 %collective-permute-done.27.refs_1_ = bf16[2,528,256]{2,1,0:T(8,128)(2,1)S(1)} collective-permute-done((bf16[2,528,256]{2,1,0:T(8,128)(2,1)S(1)}, bf16[2,528,256]{2,1,0:T(8,128)(2,1)S(1)}, u32[]{:S(2)}, u32[]{:S(2)}) %collective-permute-start.27) | collective-permute-done | bytes 540704 | tf_op jit(solution)/shard_map/ppermute | solution.py:40
  189.3 2.0 place.5
  191.3 1.7 collective-permute-done.22.refs_1_
  193.0 2.0 place.6
  195.0 1.6 place.7
  196.6 1.6 place.8
  198.2 2.0 place.9
  (82 shorter events, 4.6 us)
Async XLA Ops:
  0.6 16.0 %collective-permute-start.1 = (bf16[256,1024]{1,0:T(8,128)(2,1)}, bf16[256,1024]{1,0:T(8,128)(2,1)S(1)}, u32[]{:S(2)}, u32[]{:S(2)}) collective-permute-start(bf16[256,1024]{1,0:T(8,128)(2,1)} %refs_0_.5), channel_id=1, source_target_pairs={{0,2},{2,0},{1,3},{3,1},{4,6},{6,4},{5,7},{7,5},{8,10},{10,8},{9,1... | collective-permute-start | bytes 1572872 | tf_op jit(solution)/shard_map/ppermute | solution.py:40
  7.5 19.5 %collective-permute-start.4 = (bf16[256,1024]{1,0:T(8,128)(2,1)}, bf16[256,1024]{1,0:T(8,128)(2,1)S(1)}, u32[]{:S(2)}, u32[]{:S(2)}) collective-permute-start(bf16[256,1024]{1,0:T(8,128)(2,1)} %refs_4_.1), channel_id=1, source_target_pairs={{0,2},{2,0},{1,3},{3,1},{4,6},{6,4},{5,7},{7,5},{8,10},{10,8},{9,1... | collective-permute-start | bytes 1572872 | tf_op jit(solution)/shard_map/ppermute | solution.py:40
  7.5 19.5 %collective-permute-start = (bf16[256,1024]{1,0:T(8,128)(2,1)}, bf16[256,1024]{1,0:T(8,128)(2,1)S(1)}, u32[]{:S(2)}, u32[]{:S(2)}) collective-permute-start(bf16[256,1024]{1,0:T(8,128)(2,1)} %refs_0_.5), channel_id=1, source_target_pairs={{0,1},{1,0},{2,3},{3,2},{4,5},{5,4},{6,7},{7,6},{8,9},{9,8},{10,11... | collective-permute-start | bytes 1572872 | tf_op jit(solution)/shard_map/ppermute | solution.py:40
  16.6 10.4 %copy-start.2 = (bf16[256,1024]{1,0:T(8,128)(2,1)}, bf16[256,1024]{1,0:T(8,128)(2,1)S(1)}, u32[]{:S(2)}) copy-start(bf16[256,1024]{1,0:T(8,128)(2,1)S(1)} %collective-permute-done.1.refs_2_) | copy-start | bytes 1572868
  16.7 10.4 %collective-permute-start.2 = (bf16[256,1024]{1,0:T(8,128)(2,1)S(1)}, bf16[256,1024]{1,0:T(8,128)(2,1)S(1)}, u32[]{:S(2)}, u32[]{:S(2)}) collective-permute-start(bf16[256,1024]{1,0:T(8,128)(2,1)S(1)} %collective-permute-done.1.refs_2_), channel_id=1, source_target_pairs={{0,1},{1,0},{2,3},{3,2},{4,5},{5,4},{6,7},{7,6},{8,9},{9,8},{10,11... | collective-permute-start | bytes 1572872 | tf_op jit(solution)/shard_map/ppermute | solution.py:40
  16.7 26.1 %collective-permute-start.3 = (bf16[256,1024]{1,0:T(8,128)(2,1)}, bf16[256,1024]{1,0:T(8,128)(2,1)S(1)}, u32[]{:S(2)}, u32[]{:S(2)}) collective-permute-start(bf16[256,1024]{1,0:T(8,128)(2,1)} %refs_4_.1), channel_id=1, source_target_pairs={{0,1},{1,0},{2,3},{3,2},{4,5},{5,4},{6,7},{7,6},{8,9},{9,8},{10,11... | collective-permute-start | bytes 1572872 | tf_op jit(solution)/shard_map/ppermute | solution.py:40
  27.0 15.7 %copy-start.3 = (bf16[256,1024]{1,0:T(8,128)(2,1)}, bf16[256,1024]{1,0:T(8,128)(2,1)S(1)}, u32[]{:S(2)}) copy-start(bf16[256,1024]{1,0:T(8,128)(2,1)S(1)} %collective-permute-done.4.refs_6_) | copy-start | bytes 1572868
  27.0 15.8 %collective-permute-start.5 = (bf16[256,1024]{1,0:T(8,128)(2,1)S(1)}, bf16[256,1024]{1,0:T(8,128)(2,1)S(1)}, u32[]{:S(2)}, u32[]{:S(2)}) collective-permute-start(bf16[256,1024]{1,0:T(8,128)(2,1)S(1)} %collective-permute-done.4.refs_6_), channel_id=1, source_target_pairs={{0,1},{1,0},{2,3},{3,2},{4,5},{5,4},{6,7},{7,6},{8,9},{9,8},{10,11... | collective-permute-start | bytes 1572872 | tf_op jit(solution)/shard_map/ppermute | solution.py:40
  27.0 0.8 copy-start.4
  27.1 1.0 copy-start.5
  42.8 0.8 copy-start.6
  42.8 1.0 copy-start.7
  57.0 15.1 %copy-start.13 = (f32[6,352]{1,0:T(8,128)S(1)}, f32[6,352]{1,0:T(8,128)}, u32[]{:S(2)}) copy-start(f32[6,352]{1,0:T(8,128)} %get-tuple-element.81) | copy-start | bytes 25348
  57.0 34.6 %collective-permute-start.8 = (bf16[2,528,256]{2,1,0:T(8,128)(2,1)}, bf16[2,528,256]{2,1,0:T(8,128)(2,1)S(1)}, u32[]{:S(2)}, u32[]{:S(2)}) collective-permute-start(bf16[2,528,256]{2,1,0:T(8,128)(2,1)} %get-tuple-element.58), channel_id=1, source_target_pairs={{0,8},{4,12},{8,0},{12,4},{16,24},{20,28},{24,16},{28,20},{1,9},{5... | collective-permute-start | bytes 1622024 | tf_op jit(solution)/shard_map/ppermute | solution.py:40
  72.9 8.7 %collective-permute-start.28 = (f32[6,704]{1,0:T(8,128)S(1)}, f32[6,704]{1,0:T(8,128)S(1)}, u32[]{:S(2)}, u32[]{:S(2)}) collective-permute-start(f32[6,704]{1,0:T(8,128)S(1)} %pad_maximum_fusion.4), channel_id=1, source_target_pairs={{0,4},{4,0},{8,12},{12,8},{16,20},{20,16},{24,28},{28,24},{1,5},{5... | collective-permute-start | bytes 50696 | tf_op jit(solution)/shard_map/ppermute | solution.py:40
  74.4 20.0 %collective-permute-start.13 = (bf16[2,528,256]{2,1,0:T(8,128)(2,1)}, bf16[2,528,256]{2,1,0:T(8,128)(2,1)S(1)}, u32[]{:S(2)}, u32[]{:S(2)}) collective-permute-start(bf16[2,528,256]{2,1,0:T(8,128)(2,1)} %get-tuple-element.60), channel_id=1, source_target_pairs={{0,4},{4,0},{8,12},{12,8},{16,20},{20,16},{24,28},{28,24},{1,5},{5... | collective-permute-start | bytes 1622024 | tf_op jit(solution)/shard_map/ppermute | solution.py:40
  74.9 20.1 %collective-permute-start.18 = (bf16[2,528,256]{2,1,0:T(8,128)(2,1)}, bf16[2,528,256]{2,1,0:T(8,128)(2,1)S(1)}, u32[]{:S(2)}, u32[]{:S(2)}) collective-permute-start(bf16[2,528,256]{2,1,0:T(8,128)(2,1)} %get-tuple-element.62), channel_id=1, source_target_pairs={{0,8},{4,12},{8,0},{12,4},{16,24},{20,28},{24,16},{28,20},{1,9},{5... | collective-permute-start | bytes 1622024 | tf_op jit(solution)/shard_map/ppermute | solution.py:40
  75.1 6.4 %copy-start.14 = (f32[6,352]{1,0:T(8,128)S(1)}, f32[6,352]{1,0:T(8,128)}, u32[]{:S(2)}) copy-start(f32[6,352]{1,0:T(8,128)} %get-tuple-element.80) | copy-start | bytes 25348
  81.6 8.4 %copy-start.15 = (bf16[2,528,256]{2,1,0:T(8,128)(2,1)S(1)}, bf16[2,528,256]{2,1,0:T(8,128)(2,1)}, u32[]{:S(2)}) copy-start(bf16[2,528,256]{2,1,0:T(8,128)(2,1)} %get-tuple-element.64) | copy-start | bytes 1622020
  81.6 10.0 %copy-start.8 = (bf16[2,256,1024]{2,1,0:T(8,128)(2,1)S(1)}, bf16[2,256,1024]{2,1,0:T(8,128)(2,1)}, u32[]{:S(2)}) copy-start(bf16[2,256,1024]{2,1,0:T(8,128)(2,1)} %input_part.3) | copy-start | bytes 3145732
  81.6 12.7 %copy-start.12 = (bf16[2,528,256]{2,1,0:T(8,128)(2,1)S(1)}, bf16[2,528,256]{2,1,0:T(8,128)(2,1)}, u32[]{:S(2)}) copy-start(bf16[2,528,256]{2,1,0:T(8,128)(2,1)} %get-tuple-element.57) | copy-start | bytes 1622020
  81.6 13.3 %copy-start.11 = (bf16[2,528,256]{2,1,0:T(8,128)(2,1)S(1)}, bf16[2,528,256]{2,1,0:T(8,128)(2,1)}, u32[]{:S(2)}) copy-start(bf16[2,528,256]{2,1,0:T(8,128)(2,1)} %get-tuple-element.59) | copy-start | bytes 1622020
  81.6 14.0 %copy-start.10 = (bf16[2,528,256]{2,1,0:T(8,128)(2,1)S(1)}, bf16[2,528,256]{2,1,0:T(8,128)(2,1)}, u32[]{:S(2)}) copy-start(bf16[2,528,256]{2,1,0:T(8,128)(2,1)} %get-tuple-element.61) | copy-start | bytes 1622020
  81.6 25.1 %copy-start.9 = (bf16[2,528,256]{2,1,0:T(8,128)(2,1)S(1)}, bf16[2,528,256]{2,1,0:T(8,128)(2,1)}, u32[]{:S(2)}) copy-start(bf16[2,528,256]{2,1,0:T(8,128)(2,1)} %get-tuple-element.63) | copy-start | bytes 1622020
  81.6 9.9 %collective-permute-start.29 = (f32[6,704]{1,0:T(8,128)S(1)}, f32[6,704]{1,0:T(8,128)S(1)}, u32[]{:S(2)}, u32[]{:S(2)}) collective-permute-start(f32[6,704]{1,0:T(8,128)S(1)} %fusion.12), channel_id=1, source_target_pairs={{0,8},{4,12},{8,0},{12,4},{16,24},{20,28},{24,16},{28,20},{1,9},{5... | collective-permute-start | bytes 50696 | tf_op jit(solution)/shard_map/ppermute | solution.py:40
  90.0 15.2 %collective-permute-start.23 = (bf16[2,528,256]{2,1,0:T(8,128)(2,1)S(1)}, bf16[2,528,256]{2,1,0:T(8,128)(2,1)S(1)}, u32[]{:S(2)}, u32[]{:S(2)}) collective-permute-start(bf16[2,528,256]{2,1,0:T(8,128)(2,1)S(1)} %copy-done.15), channel_id=1, source_target_pairs={{0,4},{4,0},{8,12},{12,8},{16,20},{20,16},{24,28},{28,24},{1,5},{5... | collective-permute-start | bytes 1622024 | tf_op jit(solution)/shard_map/ppermute | solution.py:40
  91.6 31.5 %collective-permute-start.6 = (bf16[2,256,1024]{2,1,0:T(8,128)(2,1)S(1)}, bf16[2,256,1024]{2,1,0:T(8,128)(2,1)S(1)}, u32[]{:S(2)}, u32[]{:S(2)}) collective-permute-start(bf16[2,256,1024]{2,1,0:T(8,128)(2,1)S(1)} %copy-done.8), channel_id=1, source_target_pairs={{0,1},{1,0},{2,3},{3,2},{4,5},{5,4},{6,7},{7,6},{8,9},{9,8},{10,11... | collective-permute-start | bytes 3145736 | tf_op jit(solution)/shard_map/ppermute | solution.py:40
  91.6 79.0 %collective-permute-start.30 = (f32[6,704]{1,0:T(8,128)S(1)}, f32[6,704]{1,0:T(8,128)S(1)}, u32[]{:S(2)}, u32[]{:S(2)}) collective-permute-start(f32[6,704]{1,0:T(8,128)S(1)} %add.117), channel_id=1, source_target_pairs={{0,16},{4,20},{8,24},{12,28},{16,0},{20,4},{24,8},{28,12},{1,17},{... | collective-permute-start | bytes 50696 | tf_op jit(solution)/shard_map/ppermute | solution.py:40
  94.3 16.6 %collective-permute-start.9 = (bf16[528,256]{1,0:T(8,128)(2,1)S(1)}, bf16[528,256]{1,0:T(8,128)(2,1)S(1)}, u32[]{:S(2)}, u32[]{:S(2)}) collective-permute-start(bf16[528,256]{1,0:T(8,128)(2,1)S(1)} %fusion.8), channel_id=1, source_target_pairs={{0,4},{4,0},{8,12},{12,8},{16,20},{20,16},{24,28},{28,24},{1,5},{5... | collective-permute-start | bytes 811016 | tf_op jit(solution)/shard_map/ppermute | solution.py:40
  95.0 16.5 %collective-permute-start.14 = (bf16[528,256]{1,0:T(8,128)(2,1)S(1)}, bf16[528,256]{1,0:T(8,128)(2,1)S(1)}, u32[]{:S(2)}, u32[]{:S(2)}) collective-permute-start(bf16[528,256]{1,0:T(8,128)(2,1)S(1)} %fusion.9), channel_id=1, source_target_pairs={{0,8},{4,12},{8,0},{12,4},{16,24},{20,28},{24,16},{28,20},{1,9},{5... | collective-permute-start | bytes 811016 | tf_op jit(solution)/shard_map/ppermute | solution.py:40
  95.6 28.0 %copy-start.1 = (f32[2,256,1024]{2,1,0:T(8,128)S(1)}, f32[2,256,1024]{2,1,0:T(8,128)}, u32[]{:S(2)}) copy-start(f32[2,256,1024]{2,1,0:T(8,128)} %input_part.2) | copy-start | bytes 6291460
  105.2 9.7 %collective-permute-start.19 = (bf16[528,256]{1,0:T(8,128)(2,1)S(1)}, bf16[528,256]{1,0:T(8,128)(2,1)S(1)}, u32[]{:S(2)}, u32[]{:S(2)}) collective-permute-start(bf16[528,256]{1,0:T(8,128)(2,1)S(1)} %fusion.10), channel_id=1, source_target_pairs={{0,4},{4,0},{8,12},{12,8},{16,20},{20,16},{24,28},{28,24},{1,5},{5... | collective-permute-start | bytes 811016 | tf_op jit(solution)/shard_map/ppermute | solution.py:40
  111.0 9.5 %collective-permute-start.24 = (bf16[528,256]{1,0:T(8,128)(2,1)S(1)}, bf16[528,256]{1,0:T(8,128)(2,1)S(1)}, u32[]{:S(2)}, u32[]{:S(2)}) collective-permute-start(bf16[528,256]{1,0:T(8,128)(2,1)S(1)} %fusion.11), channel_id=1, source_target_pairs={{0,8},{4,12},{8,0},{12,4},{16,24},{20,28},{24,16},{28,20},{1,9},{5... | collective-permute-start | bytes 811016 | tf_op jit(solution)/shard_map/ppermute | solution.py:40
  111.5 32.2 %collective-permute-start.10 = (bf16[528,256]{1,0:T(8,128)(2,1)S(1)}, bf16[528,256]{1,0:T(8,128)(2,1)S(1)}, u32[]{:S(2)}, u32[]{:S(2)}) collective-permute-start(bf16[528,256]{1,0:T(8,128)(2,1)S(1)} %fusion.6), channel_id=1, source_target_pairs={{0,16},{4,20},{8,24},{12,28},{16,0},{20,4},{24,8},{28,12},{1,17},{... | collective-permute-start | bytes 811016 | tf_op jit(solution)/shard_map/ppermute | solution.py:40
  114.9 34.6 %collective-permute-start.15 = (bf16[528,256]{1,0:T(8,128)(2,1)S(1)}, bf16[528,256]{1,0:T(8,128)(2,1)S(1)}, u32[]{:S(2)}, u32[]{:S(2)}) collective-permute-start(bf16[528,256]{1,0:T(8,128)(2,1)S(1)} %fusion.5), channel_id=1, source_target_pairs={{0,16},{4,20},{8,24},{12,28},{16,0},{20,4},{24,8},{28,12},{1,17},{... | collective-permute-start | bytes 811016 | tf_op jit(solution)/shard_map/ppermute | solution.py:40
  120.5 34.9 %collective-permute-start.20 = (bf16[528,256]{1,0:T(8,128)(2,1)S(1)}, bf16[528,256]{1,0:T(8,128)(2,1)S(1)}, u32[]{:S(2)}, u32[]{:S(2)}) collective-permute-start(bf16[528,256]{1,0:T(8,128)(2,1)S(1)} %fusion.4), channel_id=1, source_target_pairs={{0,16},{4,20},{8,24},{12,28},{16,0},{20,4},{24,8},{28,12},{1,17},{... | collective-permute-start | bytes 811016 | tf_op jit(solution)/shard_map/ppermute | solution.py:40
  123.0 35.3 %collective-permute-start.25 = (bf16[528,256]{1,0:T(8,128)(2,1)S(1)}, bf16[528,256]{1,0:T(8,128)(2,1)S(1)}, u32[]{:S(2)}, u32[]{:S(2)}) collective-permute-start(bf16[528,256]{1,0:T(8,128)(2,1)S(1)} %fusion.3), channel_id=1, source_target_pairs={{0,16},{4,20},{8,24},{12,28},{16,0},{20,4},{24,8},{28,12},{1,17},{... | collective-permute-start | bytes 811016 | tf_op jit(solution)/shard_map/ppermute | solution.py:40
  143.7 29.1 %collective-permute-start.7 = (bf16[1,256,1024]{2,1,0:T(8,128)(2,1)S(1)}, bf16[1,256,1024]{2,1,0:T(8,128)(2,1)S(1)}, u32[]{:S(2)}, u32[]{:S(2)}) collective-permute-start(bf16[1,256,1024]{2,1,0:T(8,128)(2,1)S(1)} %fusion), channel_id=1, source_target_pairs={{0,2},{2,0},{1,3},{3,1},{4,6},{6,4},{5,7},{7,5},{8,10},{10,8},{9,1... | collective-permute-start | bytes 1572872 | tf_op jit(solution)/shard_map/ppermute | solution.py:40
  149.5 10.4 %collective-permute-start.11 = (bf16[528,256]{1,0:T(8,128)(2,1)S(1)}, bf16[528,256]{1,0:T(8,128)(2,1)S(1)}, u32[]{:S(2)}, u32[]{:S(2)}) collective-permute-start(bf16[528,256]{1,0:T(8,128)(2,1)S(1)} %add_convert_fusion.6), channel_id=1, source_target_pairs={{0,4},{4,0},{8,12},{12,8},{16,20},{20,16},{24,28},{28,24},{1,5},{5... | collective-permute-start | bytes 811016 | tf_op jit(solution)/shard_map/ppermute | solution.py:40
  155.4 9.4 %collective-permute-start.16 = (bf16[528,256]{1,0:T(8,128)(2,1)S(1)}, bf16[528,256]{1,0:T(8,128)(2,1)S(1)}, u32[]{:S(2)}, u32[]{:S(2)}) collective-permute-start(bf16[528,256]{1,0:T(8,128)(2,1)S(1)} %add_convert_fusion.4), channel_id=1, source_target_pairs={{0,8},{4,12},{8,0},{12,4},{16,24},{20,28},{24,16},{28,20},{1,9},{5... | collective-permute-start | bytes 811016 | tf_op jit(solution)/shard_map/ppermute | solution.py:40
  158.3 6.5 %collective-permute-start.21 = (bf16[528,256]{1,0:T(8,128)(2,1)S(1)}, bf16[528,256]{1,0:T(8,128)(2,1)S(1)}, u32[]{:S(2)}, u32[]{:S(2)}) collective-permute-start(bf16[528,256]{1,0:T(8,128)(2,1)S(1)} %add_convert_fusion.2), channel_id=1, source_target_pairs={{0,4},{4,0},{8,12},{12,8},{16,20},{20,16},{24,28},{28,24},{1,5},{5... | collective-permute-start | bytes 811016 | tf_op jit(solution)/shard_map/ppermute | solution.py:40
  159.9 10.6 %collective-permute-start.26 = (bf16[528,256]{1,0:T(8,128)(2,1)S(1)}, bf16[528,256]{1,0:T(8,128)(2,1)S(1)}, u32[]{:S(2)}, u32[]{:S(2)}) collective-permute-start(bf16[528,256]{1,0:T(8,128)(2,1)S(1)} %add_convert_fusion), channel_id=1, source_target_pairs={{0,8},{4,12},{8,0},{12,4},{16,24},{20,28},{24,16},{28,20},{1,9},{5... | collective-permute-start | bytes 811016 | tf_op jit(solution)/shard_map/ppermute | solution.py:40
  164.7 33.4 %collective-permute-start.12 = (bf16[2,528,256]{2,1,0:T(8,128)(2,1)S(1)}, bf16[2,528,256]{2,1,0:T(8,128)(2,1)S(1)}, u32[]{:S(2)}, u32[]{:S(2)}) collective-permute-start(bf16[2,528,256]{2,1,0:T(8,128)(2,1)S(1)} %pad_maximum_fusion.refs_0_), channel_id=1, source_target_pairs={{0,8},{4,12},{8,0},{12,4},{16,24},{20,28},{24,16},{28,20},{1,9},{5... | collective-permute-start | bytes 1622024 | tf_op jit(solution)/shard_map/ppermute | solution.py:40
  164.7 24.6 %copy-start = (s32[2]{0:T(128)S(1)}, s32[2]{0:T(128)}, u32[]{:S(2)}) copy-start(s32[2]{0:T(128)} %pad_add_fusion.me_ref.where_ref) | copy-start | bytes 28
  164.8 31.8 %collective-permute-start.17 = (bf16[2,528,256]{2,1,0:T(8,128)(2,1)S(1)}, bf16[2,528,256]{2,1,0:T(8,128)(2,1)S(1)}, u32[]{:S(2)}, u32[]{:S(2)}) collective-permute-start(bf16[2,528,256]{2,1,0:T(8,128)(2,1)S(1)} %pad_maximum_fusion.1.refs_0_), channel_id=1, source_target_pairs={{0,4},{4,0},{8,12},{12,8},{16,20},{20,16},{24,28},{28,24},{1,5},{5... | collective-permute-start | bytes 1622024 | tf_op jit(solution)/shard_map/ppermute | solution.py:40
  170.5 22.5 %collective-permute-start.22 = (bf16[2,528,256]{2,1,0:T(8,128)(2,1)S(1)}, bf16[2,528,256]{2,1,0:T(8,128)(2,1)S(1)}, u32[]{:S(2)}, u32[]{:S(2)}) collective-permute-start(bf16[2,528,256]{2,1,0:T(8,128)(2,1)S(1)} %pad_maximum_fusion.2.refs_0_), channel_id=1, source_target_pairs={{0,8},{4,12},{8,0},{12,4},{16,24},{20,28},{24,16},{28,20},{1,9},{5... | collective-permute-start | bytes 1622024 | tf_op jit(solution)/shard_map/ppermute | solution.py:40
  170.6 18.7 %collective-permute-start.27 = (bf16[2,528,256]{2,1,0:T(8,128)(2,1)S(1)}, bf16[2,528,256]{2,1,0:T(8,128)(2,1)S(1)}, u32[]{:S(2)}, u32[]{:S(2)}) collective-permute-start(bf16[2,528,256]{2,1,0:T(8,128)(2,1)S(1)} %pad_maximum_fusion.3.refs_0_), channel_id=1, source_target_pairs={{0,4},{4,0},{8,12},{12,8},{16,20},{20,16},{24,28},{28,24},{1,5},{5... | collective-permute-start | bytes 1622024 | tf_op jit(solution)/shard_map/ppermute | solution.py:40
